TPU v7x, 512 devices: a whole 4x8x8 slice. The times are simulated.
512 devices in a mesh: sp: 64 (over z, y), tp: 8 (over x, core).
Axes of the slice: x: 4, y: 8, z: 8, core: 2. Of those that a mesh axis runs over, the one named last changes fastest.
Arguments:
- tokens_in: bfloat16 [16384, 2048], P('sp', 'tp'), may hold values from -400 to 400
- norm_gain: float32 [2048], replicated, may hold values from 0.1 to 1.9
- w_query: bfloat16 [2048, 1024], P('sp', 'tp'), may hold values from -0.125 to 0.125
- w_forget: bfloat16 [2048, 1024], P('sp', 'tp'), may hold values from -0.125 to 0.125
- w_input: bfloat16 [2048, 1024], P('sp', 'tp'), may hold values from -0.125 to 0.125
- w_rgate: bfloat16 [2048, 1024], P('sp', 'tp'), may hold values from -0.125 to 0.125
- w_pool_in: bfloat16 [2048, 1024], P('sp', 'tp'), may hold values from -0.125 to 0.125
- w_pgate: bfloat16 [2048, 1024], P('sp', 'tp'), may hold values from -0.125 to 0.125
- floor_rate: float32 [1024], P('tp'), as said below
- extra_logdecay: float32 [16384, 8], P('sp', 'tp'), as said below
- state_gain: float32 [1024], P('tp'), may hold values from 0.1 to 1.9
- pool_mix: bfloat16 [8, 128, 128], P('tp'), may hold values from -0.5 to 0.5
- pool_gain: float32 [1024], P('tp'), may hold values from 0.1 to 1.9
- out_rec: bfloat16 [1024, 2048], P('tp', 'sp'), may hold values from -0.125 to 0.125
- out_pool: bfloat16 [1024, 2048], P('tp', 'sp'), may hold values from -0.125 to 0.125
- post_gain: float32 [2048], replicated, may hold values from 0.1 to 1.9
Outputs:
- mixed_out: bfloat16 [16384, 2048], P(('sp', 'tp'))
Inputs may be any that keep to these rules, and one draw needn't show every extreme that they name: `floor_rate`: every entry is positive. `extra_logdecay`: every entry is at most zero.
All inputs are finite; a program needn't handle non-finite values.
Results may differ from a plain program's by a relative error of at most 0.015.
Values may be sent and summed in bfloat16 or wider, within the bound.
A program may use at most 64 MiB of HBM per device.

v0:
```python
import jax
import jax.numpy as jnp
from jax import lax
from jax.sharding import Mesh
from jax.sharding import PartitionSpec as P

DK = 128
BLOCK = 64
SP = ("sp_0", "sp_1")
TP = ("tp_0", "tp_1")
SP_TP = ("sp_0", "sp_1", "tp_0", "tp_1")


eps = 1e-06
coarsest_scale_depth = lax.Precision.HIGHEST


def in_one_piece(arrays, axis, dim, along):
    widths = [a.shape[along] for a in arrays]
    both = jnp.concatenate(arrays, axis=along)
    out = lax.all_gather(both, axis, axis=dim, tiled=True)
    return tuple(jnp.split(out, [sum(widths[:k]) for k in range(1, len(widths))], axis=along))


def cut_rows(length, count):
    turn = length // count
    if turn >= 8:
        turn -= turn % 8
    return [turn * k for k in range(1, count)]


def all_blocks(shard, axes, order):
    tiles = shard[None]
    for k in order:
        tiles = lax.all_gather(tiles, axes[k], axis=0, tiled=True)
    held = [lax.axis_size(axes[k]) for k in reversed(order)]
    tiles = tiles.reshape(*held, *shard.shape)
    turned = sorted(range(len(order)), key=lambda place: order[len(order) - 1 - place])
    return tiles.transpose(*turned, *range(len(order), tiles.ndim)).reshape(-1, *shard.shape)


def joined_along(tiles, dim):
    tiles = jnp.moveaxis(tiles, 0, dim)
    lengths = tiles.shape
    return tiles.reshape(*lengths[:dim], lengths[dim] * lengths[dim + 1], *lengths[dim + 2 :])


def gather_at_once(shard, axes, dim):
    widest = max(range(max(1, shard.ndim - 1)), key=lambda d: shard.shape[d])
    count, done = (len(axes), [])
    for initial, piece in enumerate(
        jnp.split(shard, cut_rows(shard.shape[widest], count), axis=widest)
    ):
        if piece.size:
            order = [(initial - k) % count for k in range(count)]
            done.append(all_blocks(piece, axes, order))
    return joined_along(jnp.concatenate(done, axis=widest + 1), dim)


def nothing_yet(shard, identity):
    return jax.tree.map(
        lambda part, zero: jnp.zeros_like(part) + jnp.asarray(zero, part.dtype), shard, identity
    )


def all_in_one(shard, axis):
    leaves = jax.tree.leaves(shard)
    order = sorted(range(len(leaves)), key=lambda k: -leaves[k].size)
    width = (1, *leaves[order[0]].shape)[-1]
    lines = [
        jnp.pad(leaves[k].reshape(-1), (0, -leaves[k].size % width)).reshape(-1, width)
        for k in order
    ]
    both, at, found = (lax.all_gather(jnp.concatenate(lines), axis), 0, {})
    for k, line in zip(order, lines):
        piece = both[:, at : at + len(line)].reshape(len(both), -1)
        found[k] = piece[:, : leaves[k].size].reshape(-1, *leaves[k].shape)
        at += len(line)
    numbers = iter(range(len(leaves)))
    return jax.tree.map(lambda _: found[next(numbers)], shard)


def prefix_by_axis(shard, axes, combine, identity):
    before = start = nothing_yet(shard, identity)
    so_far = shard
    for axis in reversed(axes):
        peers, index = (lax.axis_size(axis), lax.axis_index(axis))
        pieces = all_in_one(so_far, axis)
        inside, so_far = (start, start)
        for k in range(peers):
            passed = k < index
            so_far = combine(so_far, jax.tree.map(lambda part: part[k], pieces))
            inside = jax.tree.map(lambda new, old: jnp.where(passed, new, old), so_far, inside)
        before = combine(inside, before)
    return before


def shifted(value, axis, steps):
    count = lax.axis_size(axis)
    initial, last = (max(0, -steps), min(count, count - steps))
    return lax.ppermute(value, axis, [(source, source + steps) for source in range(initial, last)])


def gather_turned(arrays, axis, dims):
    turned = [jnp.moveaxis(a, dim, 0) for a, dim in zip(arrays, dims)]
    widths = [t[0].size for t in turned]
    both = jnp.concatenate([t.reshape(-1, w) for t, w in zip(turned, widths)], axis=1)
    out = lax.all_gather(both, axis, axis=0, tiled=True)
    tiles = jnp.split(out, [sum(widths[:k]) for k in range(1, len(widths))], axis=1)
    return tuple(
        (
            jnp.moveaxis(b.reshape(-1, *t.shape[1:]), 0, dim)
            for b, t, dim in zip(tiles, turned, dims)
        )
    )


def chain_merge(earlier, later):
    return (earlier[0] * later[0], later[0][..., None] * earlier[1] + later[1])


def local_blocks(qs, keys, values, logs):
    causal = jnp.arange(BLOCK)[:, None] >= jnp.arange(BLOCK)[None, :]
    heads_dev = qs.shape[1]

    def advance(carry, member):
        carried_memory_matrix, start = carry
        probe_segment, key_piece, input_piece, gc = member
        prefix_sum_vector = jnp.cumsum(gc, axis=1)
        last_index = prefix_sum_vector[:, -1]
        cross_segment_contribution = jnp.einsum(
            "abz,azy->aby",
            probe_segment * jnp.exp(prefix_sum_vector),
            carried_memory_matrix,
            precision=coarsest_scale_depth,
        )
        diff = prefix_sum_vector[:, :, None, :] - prefix_sum_vector[:, None, :, :]
        weight = jnp.where(causal[None, :, :, None], jnp.exp(jnp.minimum(diff, 0.0)), 0.0)
        scores = jnp.einsum(
            "htk,hsk,htsk->hts", probe_segment, key_piece, weight, precision=coarsest_scale_depth
        )
        final_result = cross_segment_contribution + jnp.einsum(
            "hts,hsv->htv", scores, input_piece, precision=coarsest_scale_depth
        )
        carried_memory_matrix = jnp.exp(last_index)[..., None] * carried_memory_matrix + jnp.einsum(
            "njp,njq->npq",
            key_piece * jnp.exp(last_index[:, None, :] - prefix_sum_vector),
            input_piece,
            precision=coarsest_scale_depth,
        )
        pool_reach = probe_segment * jnp.exp(start[:, None, :] + prefix_sum_vector)
        return ((carried_memory_matrix, start + last_index), (final_result, pool_reach))

    begin = (jnp.zeros((heads_dev, DK, DK), jnp.float32), jnp.zeros((heads_dev, DK), jnp.float32))
    (carried_memory_matrix, total), (final_result, pool_reach) = lax.scan(
        advance, begin, (qs, keys, values, logs)
    )
    return (carried_memory_matrix, total, final_result, pool_reach)


def per_device(
    tokens_in,
    norm_gain,
    w_query,
    w_forget,
    w_input,
    w_rgate,
    w_pool_in,
    w_pgate,
    floor_rate,
    extra_logdecay,
    state_gain,
    pool_mix,
    pool_gain,
    out_rec,
    out_pool,
    post_gain,
):
    gathered = in_one_piece((w_query, w_forget, w_input, w_rgate, w_pool_in, w_pgate), SP, 0, 1)
    joined = jnp.concatenate(gathered, axis=1)
    head_cols = w_query.shape[1]
    positions = tokens_in.shape[0]
    model_width = norm_gain.shape[0]
    wide = gather_at_once(tokens_in, TP, 1).astype(jnp.float32)
    scaled = (wide * norm_gain[None, :]).astype(jnp.bfloat16)
    totals = jnp.dot(scaled, joined, preferred_element_type=jnp.float32)
    squares = jnp.sum(wide * wide, axis=1)
    inv_rms = lax.rsqrt(squares / model_width + eps)
    proj = (totals * inv_rms[:, None]).astype(jnp.bfloat16)
    query = proj[:, 0:head_cols]
    forget = proj[:, head_cols : 2 * head_cols]
    inputs = proj[:, 2 * head_cols : 3 * head_cols]
    rgate = proj[:, 3 * head_cols : 4 * head_cols]
    pool_in = proj[:, 4 * head_cols : 5 * head_cols]
    pgate = proj[:, 5 * head_cols : 6 * head_cols]
    heads_dev = head_cols // DK
    blocks = positions // BLOCK

    def to_blocks(array):
        return array.reshape(blocks, BLOCK, heads_dev, DK).transpose(0, 2, 1, 3)

    forget32 = forget.astype(jnp.float32)
    key_gate = -jnp.expm1(-floor_rate)[None, :] * jax.nn.sigmoid(-forget32)
    log_forget = jnp.log1p(-key_gate) + jnp.repeat(extra_logdecay, DK, axis=1)
    qs = query.astype(jnp.float32) * DK ** (-0.5)
    carried_memory_matrix, total, final_result, pool_reach = local_blocks(
        to_blocks(qs),
        to_blocks(key_gate),
        to_blocks(inputs.astype(jnp.float32)),
        to_blocks(log_forget),
    )
    decays = jnp.exp(total)
    tail_rows = pool_in[positions - 16 :]
    carried = prefix_by_axis(
        (decays, carried_memory_matrix),
        SP,
        chain_merge,
        (jnp.ones_like(decays), jnp.zeros_like(carried_memory_matrix)),
    )
    incoming_state = carried[1]
    previous = shifted(tail_rows, SP, 1).astype(jnp.float32)
    recurrent_output = final_result + jnp.einsum(
        "izaf,zfu->izau", pool_reach, incoming_state, precision=coarsest_scale_depth
    )
    grouped = recurrent_output.transpose(0, 2, 1, 3).reshape(positions, heads_dev, DK)
    normed = grouped * lax.rsqrt(jnp.mean(grouped * grouped, axis=2, keepdims=True) + eps)
    y_rec = (
        normed.reshape(positions, head_cols)
        * state_gain[None, :]
        * jax.nn.silu(rgate.astype(jnp.float32))
    ).astype(jnp.bfloat16)
    group = lax.axis_index(TP) * heads_dev + jnp.arange(head_cols) // DK
    window = jnp.power(2, 1 + group % 4).astype(jnp.int32)
    pool32 = pool_in.astype(jnp.float32)
    extended = jnp.concatenate([previous, pool32], axis=0)
    summed_rows = jnp.zeros((positions, head_cols), jnp.float32)
    for offset in range(16):
        rows_back = extended[16 - offset : 16 - offset + positions]
        summed_rows = summed_rows + jnp.where((offset < window)[None, :], rows_back, 0.0)
    place = lax.axis_index(SP) * positions + jnp.arange(positions)
    count = jnp.minimum(place[:, None] + 1, window[None, :]).astype(jnp.float32)
    mixed = (summed_rows / count - pool32).astype(jnp.bfloat16)
    mapped = jnp.einsum(
        "tgc,gcd->tgd",
        mixed.reshape(positions, heads_dev, DK),
        pool_mix,
        preferred_element_type=jnp.float32,
    ).reshape(positions, head_cols)
    y_pool = (mapped * pool_gain[None, :] * jax.nn.silu(pgate.astype(jnp.float32))).astype(
        jnp.bfloat16
    )
    out_parts = gather_turned((out_rec, out_pool), SP, (1, 1))
    both = jnp.concatenate([y_rec, y_pool], axis=1)
    weight_cat = jnp.concatenate(out_parts, axis=0)
    groups = lax.axis_size(TP)
    exchanged = lax.all_to_all(both, TP, split_axis=0, concat_axis=1, tiled=True)
    whole = lax.all_gather(weight_cat, TP, axis=0, tiled=True)
    owned = exchanged.shape[0]
    terms = jnp.einsum(
        "tjc,jcd->jtd",
        exchanged.reshape(owned, groups, 2 * head_cols),
        whole.reshape(groups, 2 * head_cols, model_width),
        preferred_element_type=jnp.float32,
    )
    summed = jnp.sum(terms.astype(jnp.bfloat16).astype(jnp.float32), axis=0)
    final = (
        summed
        * lax.rsqrt(jnp.mean(summed * summed, axis=1, keepdims=True) + eps)
        * post_gain[None, :]
    )
    return final.astype(jnp.bfloat16)


def solution(mesh):
    torus = Mesh(mesh.devices.reshape(8, 8, 4, 2), ("sp_0", "sp_1", "tp_0", "tp_1"))
    return jax.shard_map(
        per_device,
        mesh=torus,
        in_specs=(
            P(SP, TP),
            P(),
            P(SP, TP),
            P(SP, TP),
            P(SP, TP),
            P(SP, TP),
            P(SP, TP),
            P(SP, TP),
            P(TP),
            P(SP, TP),
            P(TP),
            P(TP, None, None),
            P(TP),
            P(TP, SP),
            P(TP, SP),
            P(),
        ),
        out_specs=P(SP_TP, None),
        check_vma=False,
    )
```

profile of v0, /device:TPU:1, one launch (start us, length us, event | category | flops | bytes accessed | tf_op | source)
XLA Modules:
  0.0 284.9 jit_solution(16253742989583789362)
XLA Ops:
  6.5 1.3 pad_maximum_fusion.4
  7.9 0.0 all-gather.10.cloned.1.call-start
  7.9 0.7 constant_dynamic-update-slice_fusion.5
  8.6 0.7 constant_dynamic-update-slice_fusion.4
  9.3 0.7 constant_dynamic-update-slice_fusion.3
  10.0 0.7 constant_dynamic-update-slice_fusion.2
  10.8 0.7 constant_dynamic-update-slice_fusion.1
  11.5 0.7 constant_dynamic-update-slice_fusion
  12.2 0.6 copy-done.1
  12.8 0.0 all-gather.14.cloned.1.call-start
  12.9 0.9 fusion.167
  13.7 10.5 %all-gather = bf16[512,256]{1,0:T(8,128)(2,1)S(1)} all-gather(bf16[128,256]{1,0:T(8,128)(2,1)S(1)} %get-tuple-element.199), channel_id=2, replica_groups=mesh['sp_0'=8,'sp_1'=8,'tp_0'=4,'tp_1'=2] {'tp_0'}, dimensions={0}, use_global_device_ids=true | all-gather | bytes 327680 | tf_op jit(solution)/shard_map/all_gather | solution.py:35
  24.3 10.4 %all_gather.34 = bf16[8,128,256]{2,1,0:T(8,128)(2,1)S(1)} all-gather(bf16[4,128,256]{2,1,0:T(8,128)(2,1)S(1)} %bitcast.247), channel_id=1, replica_groups=mesh['sp_0'=8,'sp_1'=8,'tp_0'=4,'tp_1'=2] {'tp_1'}, dimensions={0}, use_global_device_ids=true | all-gather | bytes 786432 | tf_op jit(solution)/shard_map/all_gather | solution.py:35
  34.7 1.9 all-gather.1
  36.8 10.3 %all_gather.36 = bf16[8,128,256]{2,1,0:T(8,128)(2,1)S(1)} all-gather(bf16[2,128,256]{2,1,0:T(8,128)(2,1)S(1)} %bitcast.249), channel_id=1, replica_groups=mesh['sp_0'=8,'sp_1'=8,'tp_0'=4,'tp_1'=2] {'tp_0'}, dimensions={0}, use_global_device_ids=true | all-gather | bytes 655360 | tf_op jit(solution)/shard_map/all_gather | solution.py:35
  47.1 0.2 convert_bitcast_fusion
  47.2 46.0 %all-gather.12.cloned.1.call-done = bf16[2048,256]{1,0:T(8,128)(2,1)} async-done(((bf16[32,256]{1,0:T(8,128)(2,1)}), bf16[2048,256]{1,0:T(8,128)(2,1)}) %all-gather.12.cloned.1.call-update) | async-done | bytes 1048592 | tf_op jit(solution)/shard_map/all_gather | solution.py:108
  93.2 1.3 slice_bitcast_fusion.2
  94.5 1.1 pad_maximum_fusion.1
  95.6 0.3 fusion.35
  96.0 1.9 copy.67
  98.1 1.9 fusion.36
  100.0 79.3 %all-gather.10.cloned.1.call-done = bf16[2048,768]{1,0:T(8,128)(2,1)} async-done(((bf16[32,768]{1,0:T(8,128)(2,1)}), bf16[2048,768]{1,0:T(8,128)(2,1)}) %all-gather.10.cloned.1.call-update) | async-done | bytes 3145744 | tf_op jit(solution)/shard_map/all_gather | solution.py:21
  179.3 2.9 %fusion.38 = bf16[256,768]{1,0:T(8,128)(2,1)S(1)} fusion(bf16[256,2048]{0,1:T(8,128)(2,1)S(1)} %fusion.36, bf16[2048,768]{1,0:T(8,128)(2,1)} %all-gather.10.cloned.1.call-done, f32[256]{0:T(256)S(1)} %add_rsqrt_fusion.1), kind=kOutput, calls=%fused_computation.54 | convolution fusion | flops 805699584 | bytes 4588544 | tf_op jit(solution)/shard_map/dot_general | solution.py:186
  182.3 2.7 collective-permute-start
  185.0 0.1 divide_multiply_fusion
  185.1 13.2 %while.17 = (s32[]{:T(128)}, f32[1,128,128]{2,1,0:T(8,128)S(1)}, f32[1,128]{1,0:T(1,128)S(1)}, f32[4,1,64,128]{3,2,1,0:T(8,128)S(1)}, f32[4,1,64,128]{3,2,1,0:T(...) while((s32[]{:T(128)}, f32[1,128,128]{2,1,0:T(8,128)S(1)}, ...), condition=%wide.region_3.4_spmd.clone, body=%wide.region_1.3_spmd.clone.sunk | while | flops 35234048 | bytes 5177500 | solution.py:155
  185.2 0.1 reduce_window_sum.16
  185.3 0.2 fusion.194
  185.5 0.3 fusion.192
  185.8 0.6 exponential_select_fusion.2
  186.5 1.7 fusion.196
  188.2 0.2 fusion.197
  188.4 0.1 reduce_window_sum.16
  188.5 0.2 fusion.194
  188.8 0.3 fusion.192
  189.1 0.6 exponential_select_fusion.2
  189.8 1.7 fusion.196
  191.5 0.2 fusion.197
  191.7 0.1 reduce_window_sum.16
  191.8 0.2 fusion.194
  192.1 0.3 fusion.192
  192.4 0.6 exponential_select_fusion.2
  193.1 1.7 fusion.196
  194.8 0.2 fusion.197
  195.0 0.1 reduce_window_sum.16
  195.1 0.2 fusion.194
  195.3 0.3 fusion.192
  195.7 0.6 exponential_select_fusion.2
  196.4 1.7 fusion.196
  198.1 0.2 fusion.197
  198.4 22.0 %all-gather.4 = f32[8,129,128]{2,1,0:T(8,128)S(1)} all-gather(f32[1,129,128]{2,1,0:T(8,128)S(1)} %maximum_bitcast_fusion), channel_id=4, replica_groups=mesh['sp_0'=8,'sp_1'=8,'tp_0'=4,'tp_1'=2] {'sp_1'}, dimensions={0}, use_global_device_ids=true | all-gather | bytes 594432 | tf_op jit(solution)/shard_map/all_gather | solution.py:74
  220.4 0.2 slice_add_fusion.8
  220.6 21.3 %all-gather.5 = f32[8,129,128]{2,1,0:T(8,128)S(1)} all-gather(f32[1,129,128]{2,1,0:T(8,128)S(1)} %maximum_bitcast_fusion.1), channel_id=5, replica_groups=mesh['sp_0'=8,'sp_1'=8,'tp_0'=4,'tp_1'=2] {'sp_0'}, dimensions={0}, use_global_device_ids=true | all-gather | bytes 594432 | tf_op jit(solution)/shard_map/all_gather | solution.py:74
  241.9 0.7 multiply_reduce_fusion.1
  242.6 0.1 rsqrt.28
  242.7 0.1 fusion.98
  242.9 0.4 fusion.41
  243.3 0.7 pad_maximum_fusion.3
  244.0 16.6 %all-to-all-start = ((bf16[8,32,256]{2,1,0:T(8,128)(2,1)}), bf16[8,32,256]{2,1,0:T(8,128)(2,1)S(1)}, u32[]{:S(2)}, u32[]{:S(2)}) async-start(bf16[8,32,256]{2,1,0:T(8,128)(2,1)} %bitcast.46), calls=%async_computation | async-start | bytes 262144 | tf_op jit(solution)/shard_map/all_to_all | solution.py:256
  260.6 11.9 %copy.74 = bf16[2048,2048]{1,0:T(8,128)(2,1)} copy(bf16[2048,2048]{0,1:T(8,128)(2,1)} %all-gather.14.cloned.1.call-done) | data formatting | bytes 16777216 | tf_op jit(solution)/shard_map/all_gather | solution.py:257
  272.5 4.9 %fusion.37 = f32[32,2048]{1,0:T(8,128)S(1)} fusion(bf16[8,256,2048]{2,1,0:T(8,128)(2,1)} %bitcast.239, bf16[8,32,256]{2,1,0:T(8,128)(2,1)S(1)} %all-to-all-done), kind=kOutput, calls=%fused_computation.52 | convolution fusion | flops 269942784 | bytes 8781824 | tf_op jit(solution)/shard_map/tjc,jcd->jtd/dot_general | solution.py:259
  277.4 0.1 multiply_reduce_fusion
  277.6 0.8 multiply_convert_fusion
  (79 shorter events, 0.8 us)
Async XLA Ops:
  6.5 236.3 %copy-start = (bf16[1,128,128]{2,1,0:T(8,128)(2,1)S(1)}, bf16[1,128,128]{2,1,0:T(8,128)(2,1)}, u32[]{:S(2)}) copy-start(bf16[1,128,128]{2,1,0:T(8,128)(2,1)} %param.29) | copy-start | bytes 98308
  6.5 86.7 %all-gather.12.cloned.1.call-start = ((), (), s32[]{:S(2)}) async-start(), calls=%async_computation.2 | async-start | bytes 1064960 | tf_op jit(solution)/shard_map/all_gather | solution.py:108
  7.9 171.4 %all-gather.10.cloned.1.call-start = ((), (), s32[]{:S(2)}) async-start(), calls=%async_computation.1 | async-start | bytes 3194880 | tf_op jit(solution)/shard_map/all_gather | solution.py:21
  12.2 0.6 copy-start.1
  12.8 247.8 %all-gather.14.cloned.1.call-start = ((), (), s32[]{:S(2)}) async-start(), calls=%async_computation.3 | async-start | bytes 9437184 | tf_op jit(solution)/shard_map/all_gather | solution.py:257
  96.0 2.1 copy-start.6
  96.0 2.1 copy-start.2
  100.0 85.0 %copy-start.4 = (f32[256,1]{0,1:T(1,128)S(1)}, f32[256,1]{0,1:T(1,128)}, u32[]{:S(2)}) copy-start(f32[256,1]{0,1:T(1,128)} %param.27) | copy-start | bytes 3076
  182.3 60.6 %collective-permute-start = (bf16[16,128]{1,0:T(8,128)(2,1)S(1)}, bf16[16,128]{1,0:T(8,128)(2,1)S(1)}, u32[]{:S(2)}, u32[]{:S(2)}) collective-permute-start(bf16[16,128]{1,0:T(8,128)(2,1)S(1)} %slice.312), channel_id=1, source_target_pairs={{0,8},{8,16},{16,24},{24,32},{32,40},{40,48},{48,56},{56,64},{64,7... | collective-permute-start | bytes 12296 | tf_op jit(solution)/shard_map/ppermute | solution.py:101
  198.3 44.4 %copy-start.5 = (f32[128]{0:T(128)S(1)}, f32[128]{0:T(128)}, u32[]{:S(2)}) copy-start(f32[128]{0:T(128)} %param.28) | copy-start | bytes 1540
  198.3 44.5 %copy-start.7 = (f32[128]{0:T(128)S(1)}, f32[128]{0:T(128)}, u32[]{:S(2)}) copy-start(f32[128]{0:T(128)} %param.30) | copy-start | bytes 1540
  244.0 28.5 %all-to-all-start = ((bf16[8,32,256]{2,1,0:T(8,128)(2,1)}), bf16[8,32,256]{2,1,0:T(8,128)(2,1)S(1)}, u32[]{:S(2)}, u32[]{:S(2)}) async-start(bf16[8,32,256]{2,1,0:T(8,128)(2,1)} %bitcast.46), calls=%async_computation | async-start | bytes 262144 | tf_op jit(solution)/shard_map/all_to_all | solution.py:256
  272.5 5.1 %copy-start.3 = (f32[2048]{0:T(1024)S(1)}, f32[2048]{0:T(1024)}, u32[]{:S(2)}) copy-start(f32[2048]{0:T(1024)} %param.33) | copy-start | bytes 24580
Sparse Core Ops, SparseCore 0:
  10.4 82.7 all-gather.11
  96.2 83.0 all-gather.9
  181.5 59.5 all-gather.13
where the time goes:
time: 286 us; the launch traced here: 285 us
  waiting for transfers between devices  125 us (44%)
  blocking collectives  76.4 us (27%)
  local copies, waits for them, and re-layouts  21.1 us (7%)
  starting transfers between devices  19.4 us (7%)
  other arithmetic  16.9 us (6%)
  between operations  13.5 us (5%)
  matrix products  11.8 us (4%)
    all_gather x1, waiting for transfers between devices, in_one_piece(): out = lax.all_gather(both, axis, axis=dim, tiled=True)  79.3 us
    all_gather x1, waiting for transfers between devices, gather_turned(): out = lax.all_gather(both, axis, axis=0, tiled=True)  46 us
    all_gather x2, blocking collectives, all_in_one(): both, at, found = (lax.all_gather(jnp.concatenate(lines), axis), 0, {})  43.3 us
    all_gather x4, blocking collectives, all_blocks(): tiles = lax.all_gather(tiles, axes[k], axis=0, tiled=True)  33.1 us
    all_to_all x1, starting transfers between devices, per_device(): lax.all_to_all(both, TP, split_axis=0, concat_axis=1, tiled=True)  16.6 us
    all_gather x1, local copies, waits for them, and re-layouts, per_device(): whole = lax.all_gather(weight_cat, TP, axis=0, tiled=True)  11.9 us
    dot_general x4, other arithmetic, advance(): jnp.einsum('htk,hsk,htsk->hts', probe_segment, key_piece, weight, precisi...  6.81 us
  transfers between devices with their start and end apart: 5, of which 2 were waited for; matrix products, arithmetic and copies ran while one was open for 15% of the time, Pallas kernels for 0%

commit v1 on v0

v1 whole, which is shorter than its diff:
```python
import functools

import jax
import jax.numpy as jnp
from jax import lax
from jax.experimental import pallas as pl
from jax.experimental.pallas import tpu as pltpu
from jax.sharding import Mesh
from jax.sharding import PartitionSpec as P

SP = ("sp_0", "sp_1")
TP = ("tp_0", "tp_1")
SP_TP = ("sp_0", "sp_1", "tp_0", "tp_1")
Z, Y, X, C = "sp_0", "sp_1", "tp_0", "tp_1"
MESH = pl.DeviceIdType.MESH
EPS = 1e-06
DK = 128
NR = 8
NX = 4
T = 256
D = 2048
OWN = T // (2 * NX)
F32 = jnp.float32
BF16 = jnp.bfloat16
ORDER = (4, 3, 5, 2, 6, 1, 7)


def mm(a, b, ca=1, cb=0):
    return lax.dot_general(a, b, (((ca,), (cb,)), ((), ())), preferred_element_type=F32)


def halves(a):
    hi = a.astype(BF16)
    return hi, (a - hi.astype(F32)).astype(BF16)


def mm3(a, b, ca=1, cb=0):
    ah, al = halves(a)
    bh, bl = halves(b)
    return mm(ah, bh, ca, cb) + (mm(ah, bl, ca, cb) + mm(al, bh, ca, cb))


def mm2(a, b, ca=1, cb=0):
    ah, al = halves(a)
    return mm(ah, b, ca, cb) + mm(al, b, ca, cb)


def silu(a):
    return a / (1.0 + jnp.exp(-a))


def around(value, count):
    return lax.rem(value + 2 * count, count)


class Ring:
    def __init__(self, part, axis, me, sign, send, recv):
        self.part, self.axis, self.me, self.sign, self.send, self.recv = part, axis, me, sign, send, recv

    def copy(self, step, back, origin):
        sign = -self.sign if back else self.sign
        at = NR // 2 + step if back else step
        block = self.part(origin)
        return pltpu.make_async_remote_copy(
            src_ref=block,
            dst_ref=block,
            send_sem=self.send.at[at],
            recv_sem=self.recv.at[at],
            device_id={self.axis: around(self.me + sign, NR)},
            device_id_type=MESH,
        )

    def origin(self, step, back):
        sign = -self.sign if back else self.sign
        return around(self.me - sign * step, NR)

    def steps(self, back):
        return NR // 2 - 1 if back else NR // 2

    def start(self, step):
        for back in (False, True):
            if step < self.steps(back):
                self.copy(step, back, self.origin(step, back)).start()

    def arrive(self, step):
        for back in (False, True):
            if step < self.steps(back):
                self.copy(step, back, self.origin(step + 1, back)).wait_recv()

    def drain(self):
        for back in (False, True):
            for step in range(self.steps(back)):
                self.copy(step, back, self.origin(step, back)).wait_send()


class Direct:
    def __init__(self, part, axis, me, send, recv):
        self.part, self.axis, self.me, self.send, self.recv = part, axis, me, send, recv

    def copy(self, distance, origin):
        block = self.part(origin)
        return pltpu.make_async_remote_copy(
            src_ref=block,
            dst_ref=block,
            send_sem=self.send.at[distance],
            recv_sem=self.recv.at[distance],
            device_id={self.axis: around(self.me + distance, NR)},
            device_id_type=MESH,
        )

    def start(self):
        for distance in ORDER:
            self.copy(distance, self.me).start()

    def arrive(self):
        for distance in range(1, NR):
            self.copy(distance, around(self.me - distance, NR)).wait_recv()

    def drain(self):
        for distance in range(1, NR):
            self.copy(distance, self.me).wait_send()


def layer(
    tok, wq, wf, wi, wr, wp, wg, orec, opool,
    ngain, rate, extra, sgain, pmix, pgain, post,
    out,
    g0a, g0b, g1a, g1b, g2a, g2b, xg, sc,
    st1, st2, rows_out, rows_in, yb, sib_out, sib_in, red_out, red_in,
    lsem, p1s, p1r, p2s, p2r, ts, tr, ss, sr, ps, pr, bs, br, xs, xr,
):
    z, y, x, c = lax.axis_index(Z), lax.axis_index(Y), lax.axis_index(X), lax.axis_index(C)
    tp = 2 * x + c
    sign = 1 - 2 * c
    other = 1 - c

    local = [
        pltpu.make_async_copy(src, dst, lsem.at[k])
        for k, (src, dst) in enumerate(
            (
                (wf, g0a.at[z, y]),
                (wi, g0b.at[z, y]),
                (tok, xg.at[tp]),
                (wq, g1a.at[z, y, :, 0:DK]),
                (wr, g1a.at[z, y, :, DK : 2 * DK]),
                (wp, g1b.at[z, y, :, 0:DK]),
                (wg, g1b.at[z, y, :, DK : 2 * DK]),
                (orec, g2a.at[z, y]),
                (opool, g2b.at[z, y]),
            )
        )
    ]
    for copy in local:
        copy.start()

    after_y = around(y + 1, NR)
    after_z = jnp.where(y == NR - 1, around(z + 1, NR), z)
    before_y = around(y - 1, NR)
    before_z = jnp.where(y == 0, around(z - 1, NR), z)
    barrier = pltpu.get_barrier_semaphore()
    for k in range(1, NR):
        pl.semaphore_signal(barrier, 1, device_id={Y: around(y + k, NR)}, device_id_type=MESH)
        pl.semaphore_signal(barrier, 1, device_id={Z: around(z + k, NR)}, device_id_type=MESH)
    for k in range(1, NX):
        pl.semaphore_signal(barrier, 1, device_id={X: around(x + k, NX)}, device_id_type=MESH)
    pl.semaphore_signal(barrier, 1, device_id={C: other}, device_id_type=MESH)
    pl.semaphore_signal(barrier, 1, device_id={Z: before_z, Y: before_y}, device_id_type=MESH)
    pl.semaphore_wait(barrier, 2 * (NR - 1) + NX - 1 + 2)

    groups = ((g0a, g0b), (g1a, g1b), (g2a, g2b))
    first, second = [], []
    for k, (ga, gb) in enumerate(groups):
        first.append(Direct(lambda o, g=ga: g.at[z, o], Y, y, p1s.at[2 * k], p1r.at[2 * k]))
        first.append(Direct(lambda o, g=gb: g.at[o, y], Z, z, p1s.at[2 * k + 1], p1r.at[2 * k + 1]))
        second.append(Ring(lambda o, g=ga: g.at[o], Z, z, sign, p2s.at[2 * k], p2r.at[2 * k]))
        second.append(
            Ring(lambda o, g=gb: g.at[:, o], Y, y, sign, p2s.at[2 * k + 1], p2r.at[2 * k + 1])
        )

    def tok_copy(at, slot, where):
        return pltpu.make_async_remote_copy(
            src_ref=xg.at[slot],
            dst_ref=xg.at[slot],
            send_sem=ts.at[at],
            recv_sem=tr.at[at],
            device_id=where,
            device_id_type=MESH,
        )

    def tok_out(distance):
        return tok_copy(distance, tp, {X: around(x + distance, NX)})

    def tok_from(distance):
        return 2 * around(x - distance, NX)

    local[0].wait()
    first[0].start()
    local[1].wait()
    first[1].start()
    local[2].wait()
    for distance in (2, 1, 3):
        tok_out(distance).start()
    tok_copy(0, tp, {C: other}).start()
    for k in range(3, 7):
        local[k].wait()
    first[2].start()
    first[3].start()

    first[0].arrive()
    second[0].start(0)
    first[1].arrive()
    second[1].start(0)
    for k in range(7, 9):
        local[k].wait()
    first[2].arrive()
    second[2].start(0)
    first[3].arrive()
    second[3].start(0)
    first[4].start()
    first[5].start()

    def relay(group, step):
        for ring in second[2 * group : 2 * group + 2]:
            ring.arrive(step)
            if step + 1 < NR // 2:
                ring.start(step + 1)

    for distance in (1, 3, 2):
        tok_copy(distance, tok_from(distance) + c, {X: around(x + distance, NX)}).wait_recv()
        tok_copy(NX + distance, tok_from(distance) + c, {C: other}).start()
    relay(0, 0)
    tok_copy(0, 2 * x + other, {C: other}).wait_recv()
    for distance in range(1, NX):
        tok_copy(NX + distance, tok_from(distance) + other, {C: other}).wait_recv()
    squares = jnp.zeros((T, 1), F32)
    for k in range(2 * NX):
        block = xg[k].astype(F32)
        squares = squares + jnp.sum(block * block, axis=1, keepdims=True)
        at = slice(k * (D // (2 * NX)), (k + 1) * (D // (2 * NX)))
        sc[:, at] = (block * ngain[:, at]).astype(BF16)
    inv_rms = lax.rsqrt(squares * (1.0 / D) + EPS)
    relay(1, 0)
    relay(0, 1)
    relay(1, 1)
    relay(0, 2)
    relay(1, 2)
    first[4].arrive()
    second[4].start(0)
    first[5].arrive()
    second[5].start(0)
    relay(0, 3)

    scaled = sc[...]
    forget = (mm(scaled, g0a[...].reshape(D, DK)) * inv_rms).astype(BF16).astype(F32)
    value = (mm(scaled, g0b[...].reshape(D, DK)) * inv_rms).astype(BF16)
    r = rate[...]
    series = r * (1.0 - r / 2 * (1.0 - r / 3 * (1.0 - r / 4 * (1.0 - r / 5 * (1.0 - r / 6)))))
    reach = jnp.where(r < 0.1, series, 1.0 - jnp.exp(-r))
    key = reach * (1.0 / (1.0 + jnp.exp(forget)))
    more = lax.dot_general(
        extra[...],
        jnp.ones((1, DK), F32),
        (((0,), (0,)), ((), ())),
        precision=lax.Precision.HIGHEST,
        preferred_element_type=F32,
    )
    logs = jnp.log1p(-key) + more
    row = lax.broadcasted_iota(jnp.int32, (T, T), 0)
    col = lax.broadcasted_iota(jnp.int32, (T, T), 1)
    lower = jnp.where(row >= col, 1.0, 0.0)
    cum = jnp.dot(lower, logs, precision=lax.Precision.HIGHEST, preferred_element_type=F32)
    last = cum[T - 1 : T, :]
    memory = mm2(key * jnp.exp(last - cum), value, 0, 0).T

    def to_message(state, total):
        hi = total.astype(BF16)
        rest = total - hi.astype(F32)
        mid = rest.astype(BF16)
        low = (rest - mid.astype(F32)).astype(BF16)
        place = lax.broadcasted_iota(jnp.int32, (16, DK), 0)
        parts = jnp.where(
            place == 0,
            hi.astype(F32),
            jnp.where(place == 1, mid.astype(F32), jnp.where(place == 2, low.astype(F32), 0.0)),
        )
        return jnp.concatenate([state.astype(BF16), parts.astype(BF16)], axis=0)

    def from_message(ref, k):
        whole = ref[k].astype(F32)
        return whole[:DK], jnp.sum(whole[DK:], axis=0, keepdims=True)

    st1[y] = to_message(memory, last)
    over_y = Direct(lambda o: st1.at[o], Y, y, ss.at[0], sr.at[0])
    over_y.start()
    relay(1, 3)

    qr = mm(scaled, g1a[...].reshape(D, 2 * DK)) * inv_rms
    query = qr[:, :DK].astype(BF16).astype(F32) * DK ** (-0.5)
    rgate = qr[:, DK:].astype(BF16).astype(F32)
    pp = mm(scaled, g1b[...].reshape(D, 2 * DK)) * inv_rms
    pool = pp[:, :DK].astype(BF16)
    pgate = pp[:, DK:].astype(BF16).astype(F32)
    rows_out[...] = pool[T - 16 :, :]
    shift = pltpu.make_async_remote_copy(
        src_ref=rows_out,
        dst_ref=rows_in,
        send_sem=ps.at[0],
        recv_sem=pr.at[0],
        device_id={Z: after_z, Y: after_y},
        device_id_type=MESH,
    )
    shift.start()
    relay(2, 0)

    value32 = value.astype(F32)
    in_block = lax.rem(lax.broadcasted_iota(jnp.int32, (T, 1), 0), 8)
    decay = jnp.exp(logs)
    weight = query
    rec = jnp.sum(query * key, axis=1, keepdims=True) * value32
    for d in range(1, 8):
        weight = weight * (decay if d == 1 else pltpu.roll(decay, d - 1, 0))
        score = jnp.sum(weight * pltpu.roll(key, d, 0), axis=1, keepdims=True)
        rec = rec + jnp.where(in_block >= d, score, 0.0) * pltpu.roll(value32, d, 0)
    relay(2, 1)
    scores = jnp.zeros((T, T), F32)
    for half in (8, 16, 32, 64, 128):
        apart = cum.reshape(T // (2 * half), 2 * half, DK)
        apart = jnp.abs(apart - apart[:, half - 1 : half, :]).reshape(T, DK)
        fade = jnp.exp(-apart)
        level = mm3(query * fade, key * fade, 1, 1)
        mask = (row // (2 * half) == col // (2 * half)) & (row // half > col // half)
        scores = jnp.where(mask, level, scores)
    rec = rec + mm2(scores, value)

    def chain(ref, place, count):
        state, total = jnp.zeros((DK, DK), F32), jnp.zeros((1, DK), F32)
        inside, before = state, total
        for k in range(count):
            new_state, new_total = from_message(ref, k)
            state = jnp.exp(new_total) * state + new_state
            total = total + new_total
            inside = jnp.where(k < place, state, inside)
            before = jnp.where(k < place, total, before)
        return state, total, inside, before

    over_y.arrive()
    state, total, inside, before = chain(st1, y, NR)
    st2[z] = to_message(state, total)
    over_z = Direct(lambda o: st2.at[o], Z, z, ss.at[1], sr.at[1])
    over_z.start()
    relay(2, 2)

    shift.wait_recv()
    at_start = (z == 0) & (y == 0)
    earlier = jnp.where(at_start, 0.0, rows_in[...].astype(F32))
    pool32 = pool.astype(F32)
    two = jnp.concatenate([earlier, pool32], axis=0)
    two = two + pltpu.roll(two, 1, 0)
    four = two + pltpu.roll(two, 2, 0)
    eight = four + pltpu.roll(four, 4, 0)
    sixteen = eight + pltpu.roll(eight, 8, 0)
    kind = lax.rem(tp, 4)
    sums = jnp.where(kind == 0, two, jnp.where(kind == 1, four, jnp.where(kind == 2, eight, sixteen)))
    width = jnp.where(kind == 0, 2, jnp.where(kind == 1, 4, jnp.where(kind == 2, 8, 16)))
    place = (z * NR + y) * T + lax.broadcasted_iota(jnp.int32, (T, 1), 0)
    count = jnp.minimum(place + 1, width).astype(F32)
    mixed = (sums[16:] / count - pool32).astype(BF16)
    y_pool = (mm(mixed, pmix[...]) * pgain[...] * silu(pgate)).astype(BF16)
    gate = sgain[...] * silu(rgate)
    faded = query * jnp.exp(cum)
    relay(2, 3)

    over_z.arrive()
    _, _, outer, _ = chain(st2, z, NR)
    incoming = jnp.exp(before) * outer + inside
    rec = rec + mm3(faded, incoming, 1, 1)
    normed = rec * lax.rsqrt(jnp.mean(rec * rec, axis=1, keepdims=True) + EPS)
    y_rec = (normed * gate).astype(BF16)

    yb[...] = jnp.concatenate([y_rec, y_pool], axis=1).reshape(NX, 2, OWN, 2 * DK)

    def project(k, parity):
        left = yb[k, parity]
        return mm(left[:, :DK], g2a[...].reshape(D, DK), 1, 1) + mm(
            left[:, DK:], g2b[...].reshape(D, DK), 1, 1
        )

    def sib_copy(k):
        return pltpu.make_async_remote_copy(
            src_ref=sib_out.at[k],
            dst_ref=sib_in.at[k],
            send_sem=bs.at[k],
            recv_sem=br.at[k],
            device_id={C: other},
            device_id_type=MESH,
        )

    theirs = yb[:, other].reshape(NX * OWN, 2 * DK)
    mine = yb[:, c].reshape(NX * OWN, 2 * DK)
    for half in range(2):
        left = theirs[half * 2 * OWN : (half + 1) * 2 * OWN]
        part = mm(left[:, :DK], g2a[...].reshape(D, DK), 1, 1) + mm(
            left[:, DK:], g2b[...].reshape(D, DK), 1, 1
        )
        for k in range(2):
            sib_out[2 * half + k] = part[k * OWN : (k + 1) * OWN].astype(BF16)
            sib_copy(2 * half + k).start()

    def red_copy(distance):
        return pltpu.make_async_remote_copy(
            src_ref=red_out.at[around(x + distance, NX)],
            dst_ref=red_in.at[distance - 1],
            send_sem=xs.at[distance - 1],
            recv_sem=xr.at[distance - 1],
            device_id={X: around(x + distance, NX)},
            device_id_type=MESH,
        )

    part = mm(mine[:, :DK], g2a[...].reshape(D, DK), 1, 1) + mm(
        mine[:, DK:], g2b[...].reshape(D, DK), 1, 1
    )
    for k in range(NX):
        sib_copy(k).wait_recv()
        red_out[k] = (part[k * OWN : (k + 1) * OWN] + sib_in[k].astype(F32)).astype(BF16)
    for distance in (2, 1, 3):
        red_copy(distance).start()
    summed = red_out[x].astype(F32)
    for distance in (1, 3, 2):
        red_copy(distance).wait_recv()
        summed = summed + red_in[distance - 1].astype(F32)
    scale = lax.rsqrt(jnp.mean(summed * summed, axis=1, keepdims=True) + EPS)
    out[...] = (summed * scale * post[...]).astype(BF16)

    for stream in first:
        stream.drain()
    for stream in second:
        stream.drain()
    over_y.drain()
    over_z.drain()
    for distance in range(1, NX):
        tok_out(distance).wait_send()
        tok_copy(NX + distance, tok_from(distance) + c, {C: other}).wait_send()
        red_copy(distance).wait_send()
    tok_copy(0, tp, {C: other}).wait_send()
    for k in range(NX):
        sib_copy(k).wait_send()
    shift.wait_send()


def per_device(
    tokens_in, norm_gain, w_query, w_forget, w_input, w_rgate, w_pool_in, w_pgate,
    floor_rate, extra_logdecay, state_gain, pool_mix, pool_gain, out_rec, out_pool, post_gain,
):
    anywhere = pl.BlockSpec(memory_space=pl.ANY)
    close = pl.BlockSpec(memory_space=pltpu.VMEM)
    dma = pltpu.SemaphoreType.DMA
    return pl.pallas_call(
        layer,
        name="layer",
        out_shape=jax.ShapeDtypeStruct((OWN, D), BF16),
        in_specs=[anywhere] * 9 + [close] * 7,
        out_specs=close,
        scratch_shapes=[
            pltpu.VMEM((NR, NR, D // 64, DK), BF16),
            pltpu.VMEM((NR, NR, D // 64, DK), BF16),
            pltpu.VMEM((NR, NR, D // 64, 2 * DK), BF16),
            pltpu.VMEM((NR, NR, D // 64, 2 * DK), BF16),
            pltpu.VMEM((NR, NR, D // 64, DK), BF16),
            pltpu.VMEM((NR, NR, D // 64, DK), BF16),
            pltpu.VMEM((2 * NX, T, D // (2 * NX)), BF16),
            pltpu.VMEM((T, D), BF16),
            pltpu.VMEM((NR, DK + 16, DK), BF16),
            pltpu.VMEM((NR, DK + 16, DK), BF16),
            pltpu.VMEM((16, DK), BF16),
            pltpu.VMEM((16, DK), BF16),
            pltpu.VMEM((NX, 2, OWN, 2 * DK), BF16),
            pltpu.VMEM((NX, OWN, D), BF16),
            pltpu.VMEM((NX, OWN, D), BF16),
            pltpu.VMEM((NX, OWN, D), BF16),
            pltpu.VMEM((NX - 1, OWN, D), BF16),
            dma((9,)),
            dma((6, NR)),
            dma((6, NR)),
            dma((6, NR)),
            dma((6, NR)),
            dma((2 * NX,)),
            dma((2 * NX,)),
            dma((2, NR)),
            dma((2, NR)),
            dma((1,)),
            dma((1,)),
            dma((NX,)),
            dma((NX,)),
            dma((NX,)),
            dma((NX,)),
        ],
        compiler_params=pltpu.CompilerParams(
            collective_id=0, has_side_effects=True, vmem_limit_bytes=56 * 1024 * 1024
        ),
    )(
        tokens_in,
        w_query,
        w_forget,
        w_input,
        w_rgate,
        w_pool_in,
        w_pgate,
        out_rec.T,
        out_pool.T,
        norm_gain.reshape(1, -1),
        floor_rate.reshape(1, -1),
        extra_logdecay.reshape(1, -1),
        state_gain.reshape(1, -1),
        pool_mix.reshape(DK, DK),
        pool_gain.reshape(1, -1),
        post_gain.reshape(1, -1),
    )


def solution(mesh):
    torus = Mesh(mesh.devices.reshape(8, 8, 4, 2), ("sp_0", "sp_1", "tp_0", "tp_1"))
    return jax.shard_map(
        per_device,
        mesh=torus,
        in_specs=(
            P(SP, TP),
            P(),
            P(SP, TP),
            P(SP, TP),
            P(SP, TP),
            P(SP, TP),
            P(SP, TP),
            P(SP, TP),
            P(TP),
            P(SP, TP),
            P(TP),
            P(TP, None, None),
            P(TP),
            P(TP, SP),
            P(TP, SP),
            P(),
        ),
        out_specs=P(SP_TP, None),
        check_vma=False,
    )
```

time: 286 us -> 78.3 us (0.27)
  waiting for transfers between devices: 125 us -> 0 us
  Pallas kernels: 0 us -> 76.5 us
  blocking collectives: 76.4 us -> 0 us
  local copies, waits for them, and re-layouts: 21.1 us -> 1.57 us
  starting transfers between devices: 19.4 us -> 0 us
  other arithmetic: 16.9 us -> 0 us
  between operations: 13.5 us -> 0.01 us
  matrix products: 11.8 us -> 0 us
    all_gather x3 -> x0, waiting for transfers between devices: 125 us -> none  [the longest x1 79.3 us: in_one_piece(): out = lax.all_gather(both, axis, axis=dim, tiled=True)]
    pallas_call x0 -> x1, Pallas kernels: none -> 76.5 us  [per_device(): pl.pallas_call(layer, name='layer', out_shape=jax.ShapeDtypeStruct((OWN,...]
    all_gather x6 -> x0, blocking collectives: 76.4 us -> none  [the longest x2 43.3 us: all_in_one(): both, at, found = (lax.all_gather(jnp.concatenate(lines), axis), 0, {})]
    all_to_all x1 -> x0, starting transfers between devices: 16.6 us -> none  [per_device(): lax.all_to_all(both, TP, split_axis=0, concat_axis=1, tiled=True)]
    all_gather x1 -> x0, local copies, waits for them, and re-layouts: 11.9 us -> none  [per_device(): whole = lax.all_gather(weight_cat, TP, axis=0, tiled=True)]
    dot_general x16 -> x0, matrix products: 11.8 us -> none  [the longest x1 4.94 us: per_device(): jnp.einsum('tjc,jcd->jtd', exchanged.reshape(owned, groups, 2 * head_cols...]
    dot_general x4 -> x0, other arithmetic: 6.81 us -> none  [advance(): jnp.einsum('htk,hsk,htsk->hts', probe_segment, key_piece, weight, precisi...]
    concatenate x3 -> x0, other arithmetic: 3.1 us -> none  [the longest x1 1.32 us: gather_turned(): jnp.concatenate([t.reshape(-1, w) for t, w in zip(turned, widths)], axis=1)]
  transfers between devices with their start and end apart: 5 -> 0, of which waited for: 2 -> 0; matrix products, arithmetic and copies ran while one was open for 15% -> 0% of each run, Pallas kernels for 0% -> 0%
where the time goes in v1:
time: 78.3 us; the launch traced here: 78.1 us
  Pallas kernels  76.5 us (98%)
  local copies, waits for them, and re-layouts  1.57 us (2%)
    pallas_call x1, Pallas kernels, per_device(): pl.pallas_call(layer, name='layer', out_shape=jax.ShapeDtypeStruct((OWN,...  76.5 us
    unnamed x1, local copies, waits for them, and re-layouts  1.57 us

profile of v1, /device:TPU:1, one launch (start us, length us, event | category | flops | bytes accessed | tf_op | source)
XLA Modules:
  0.0 78.1 jit_solution(258114135108774095)
XLA Ops:
  0.0 76.5 %layer.1 = bf16[32,2048]{1,0:T(8,128)(2,1)} custom-call(bf16[256,256]{1,0:T(8,128)(2,1)} %tok.1, bf16[32,128]{1,0:T(8,128)(2,1)} %wq.1, bf16[32,128]{1,0:T(8,128)(2,1)} %wf.1, bf16[32,128]{1,0:T(8,128)(2,1)} %wi.1, bf16[32,128]{1,0:T(8,128)(2,1)} %wr.1, bf16[32,128]{1,0:T(8,128)(2,1)} %wp.1, bf16[32,128]{1,0:T(8,128)(2,1)} %wg.1, bf16[32,128]{1,0:T(8,128)(2,1)} %bitcast.10, ...), custom_call_target="tpu_custom_call" | custom-call | tf_op jit(solution)/shard_map/layer/pallas_call | solution.py:457
  76.5 1.6 %copy.18 = bf16[32,2048]{1,0:T(8,128)(2,1)} copy(bf16[32,2048]{1,0:T(8,128)(2,1)} %layer.1) | data formatting | bytes 262144

commit v2 on v1

v2 whole, which is shorter than its diff:
```python
import functools

import jax
import jax.numpy as jnp
from jax import lax
from jax.experimental import pallas as pl
from jax.experimental.pallas import tpu as pltpu
from jax.sharding import Mesh
from jax.sharding import PartitionSpec as P

SP = ("sp_0", "sp_1")
TP = ("tp_0", "tp_1")
SP_TP = ("sp_0", "sp_1", "tp_0", "tp_1")
Z, Y, X, C = "sp_0", "sp_1", "tp_0", "tp_1"
MESH = pl.DeviceIdType.MESH
EPS = 1e-06
DK = 128
NR = 8
NX = 4
T = 256
D = 2048
OWN = T // (2 * NX)
F32 = jnp.float32
BF16 = jnp.bfloat16
ORDER = (4, 3, 5, 2, 6, 1, 7)


def mm(a, b, ca=1, cb=0):
    return lax.dot_general(a, b, (((ca,), (cb,)), ((), ())), preferred_element_type=F32)


def halves(a):
    hi = a.astype(BF16)
    return hi, (a - hi.astype(F32)).astype(BF16)


def mm3(a, b, ca=1, cb=0):
    ah, al = halves(a)
    bh, bl = halves(b)
    return mm(ah, bh, ca, cb) + (mm(ah, bl, ca, cb) + mm(al, bh, ca, cb))


def mm2(a, b, ca=1, cb=0):
    ah, al = halves(a)
    return mm(ah, b, ca, cb) + mm(al, b, ca, cb)


def silu(a):
    return a / (1.0 + jnp.exp(-a))


def around(value, count):
    return lax.rem(value + 2 * count, count)


class Ring:
    def __init__(self, part, axis, me, sign, send, recv):
        self.part, self.axis, self.me, self.sign, self.send, self.recv = part, axis, me, sign, send, recv

    def copy(self, step, back, origin):
        sign = -self.sign if back else self.sign
        at = NR // 2 + step if back else step
        block = self.part(origin)
        return pltpu.make_async_remote_copy(
            src_ref=block,
            dst_ref=block,
            send_sem=self.send.at[at],
            recv_sem=self.recv.at[at],
            device_id={self.axis: around(self.me + sign, NR)},
            device_id_type=MESH,
        )

    def origin(self, step, back):
        sign = -self.sign if back else self.sign
        return around(self.me - sign * step, NR)

    def steps(self, back):
        return NR // 2 - 1 if back else NR // 2

    def start(self, step):
        for back in (False, True):
            if step < self.steps(back):
                self.copy(step, back, self.origin(step, back)).start()

    def arrive(self, step):
        for back in (False, True):
            if step < self.steps(back):
                self.copy(step, back, self.origin(step + 1, back)).wait_recv()

    def drain(self):
        for back in (False, True):
            for step in range(self.steps(back)):
                self.copy(step, back, self.origin(step, back)).wait_send()


class Direct:
    def __init__(self, part, axis, me, send, recv):
        self.part, self.axis, self.me, self.send, self.recv = part, axis, me, send, recv

    def copy(self, distance, origin):
        block = self.part(origin)
        return pltpu.make_async_remote_copy(
            src_ref=block,
            dst_ref=block,
            send_sem=self.send.at[distance],
            recv_sem=self.recv.at[distance],
            device_id={self.axis: around(self.me + distance, NR)},
            device_id_type=MESH,
        )

    def start(self):
        for distance in ORDER:
            self.copy(distance, self.me).start()

    def arrive(self):
        for distance in range(1, NR):
            self.copy(distance, around(self.me - distance, NR)).wait_recv()

    def drain(self):
        for distance in range(1, NR):
            self.copy(distance, self.me).wait_send()


class Swap:
    def __init__(self, out, held, axis, me, send, recv):
        self.out, self.held, self.axis, self.me, self.send, self.recv = out, held, axis, me, send, recv

    def copy(self, distance, origin):
        other = around(self.me + distance, NR)
        return pltpu.make_async_remote_copy(
            src_ref=self.out.at[other],
            dst_ref=self.held.at[origin],
            send_sem=self.send.at[distance],
            recv_sem=self.recv.at[distance],
            device_id={self.axis: other},
            device_id_type=MESH,
        )

    def start(self):
        for distance in ORDER:
            self.copy(distance, self.me).start()

    def arrive(self):
        for distance in range(1, NR):
            self.copy(distance, around(self.me - distance, NR)).wait_recv()

    def drain(self):
        for distance in range(1, NR):
            self.copy(distance, self.me).wait_send()


def log_rows(total):
    hi = total.astype(BF16)
    rest = total - hi.astype(F32)
    mid = rest.astype(BF16)
    low = (rest - mid.astype(F32)).astype(BF16)
    place = lax.broadcasted_iota(jnp.int32, (16, DK), 0)
    parts = jnp.where(place == 1, mid.astype(F32), jnp.where(place == 2, low.astype(F32), 0.0))
    return jnp.where(place == 0, hi.astype(F32), parts).astype(BF16)


def from_message(ref, k):
    whole = ref[k].astype(F32)
    return whole[:16], jnp.sum(whole[16:], axis=0, keepdims=True)


def layer(
    tok, wq, wf, wi, wr, wp, wg, orec, opool,
    ngain_in, rate_in, extra_in, sgain_in, pmix_in, pgain_in, post_in,
    out,
    g0a, g0b, g1a, g1b, xg, sc,
    ngain, rate, extra, sgain, pmix, pgain, post,
    st_out, st1, st2, st3_out, st3, rows_out, rows_in, yb, sib_out, sib_in, red_out, red_in, mid_in,
    lsem, vsem, p1s, p1r, p2s, p2r, ts, tr, ss, sr, ps, pr, bs, br, xs, xr,
):
    scope = jax.named_scope
    z, y, x, c = lax.axis_index(Z), lax.axis_index(Y), lax.axis_index(X), lax.axis_index(C)
    tp = 2 * x + c
    sign = 1 - 2 * c
    other = 1 - c

    local = [
        pltpu.make_async_copy(src, dst, lsem.at[k])
        for k, (src, dst) in enumerate(
            (
                (wf, g0a.at[z, y]),
                (wi, g0b.at[z, y]),
                (tok, xg.at[tp]),
                (wq, g1a.at[0, z, y]),
                (wr, g1a.at[1, z, y]),
                (orec, g1a.at[2, z, y]),
                (wp, g1b.at[0, z, y]),
                (wg, g1b.at[1, z, y]),
                (opool, g1b.at[2, z, y]),
            )
        )
    ]
    vectors = [
        pltpu.make_async_copy(src, dst, vsem.at[k])
        for k, (src, dst) in enumerate(
            (
                (ngain_in, ngain),
                (rate_in, rate),
                (extra_in, extra),
                (sgain_in, sgain),
                (pmix_in, pmix),
                (pgain_in, pgain),
                (post_in, post),
            )
        )
    ]
    for copy in local + vectors:
        copy.start()

    after_y = around(y + 1, NR)
    after_z = jnp.where(y == NR - 1, around(z + 1, NR), z)
    before_y = around(y - 1, NR)
    before_z = jnp.where(y == 0, around(z - 1, NR), z)
    with scope("barrier"):
        barrier = pltpu.get_barrier_semaphore()
        for k in ORDER:
            pl.semaphore_signal(barrier, 1, device_id={Y: around(y + k, NR)}, device_id_type=MESH)
            pl.semaphore_signal(barrier, 1, device_id={Z: around(z + k, NR)}, device_id_type=MESH)
        for k in range(1, NX):
            pl.semaphore_signal(barrier, 1, device_id={X: around(x + k, NX)}, device_id_type=MESH)
        pl.semaphore_signal(barrier, 1, device_id={C: other}, device_id_type=MESH)
        pl.semaphore_signal(barrier, 1, device_id={Z: before_z, Y: before_y}, device_id_type=MESH)
        pl.semaphore_wait(barrier, 2 * (NR - 1) + NX - 1 + 2)

    first = [
        Direct(lambda o: g0a.at[z, o], Y, y, p1s.at[0], p1r.at[0]),
        Direct(lambda o: g0b.at[o, y], Z, z, p1s.at[1], p1r.at[1]),
        Direct(lambda o: g1a.at[:, z, o], Y, y, p1s.at[2], p1r.at[2]),
        Direct(lambda o: g1b.at[:, o, y], Z, z, p1s.at[3], p1r.at[3]),
    ]
    streams = [
        (
            Ring(lambda o: g0a.at[o], Z, z, sign, p2s.at[0], p2r.at[0]),
            Ring(lambda o: g0b.at[:, o], Y, y, sign, p2s.at[1], p2r.at[1]),
        )
    ] + [
        (
            Ring(lambda o, k=k: g1a.at[k, o], Z, z, sign, p2s.at[2 * k + 2], p2r.at[2 * k + 2]),
            Ring(lambda o, k=k: g1b.at[k, :, o], Y, y, sign, p2s.at[2 * k + 3], p2r.at[2 * k + 3]),
        )
        for k in range(3)
    ]

    def start(k, step):
        for ring in streams[k]:
            ring.start(step)

    def relay(k, step):
        with scope("relay%d%d" % (k, step)):
            for ring in streams[k]:
                ring.arrive(step)
                if step + 1 < NR // 2:
                    ring.start(step + 1)

    def tok_copy(at, slot, where):
        return pltpu.make_async_remote_copy(
            src_ref=xg.at[slot],
            dst_ref=xg.at[slot],
            send_sem=ts.at[at],
            recv_sem=tr.at[at],
            device_id=where,
            device_id_type=MESH,
        )

    def tok_out(distance):
        return tok_copy(distance, tp, {X: around(x + distance, NX)})

    def tok_from(distance):
        return 2 * around(x - distance, NX)

    with scope("sends"):
        local[0].wait()
        first[0].start()
        local[1].wait()
        first[1].start()
        local[2].wait()
        for distance in (2, 1, 3):
            tok_out(distance).start()
        tok_copy(0, tp, {C: other}).start()
        for k in range(3, 6):
            local[k].wait()
        first[2].start()
        for k in range(6, 9):
            local[k].wait()
        first[3].start()
        for copy in vectors:
            copy.wait()

    with scope("first0"):
        first[0].arrive()
        streams[0][0].start(0)
        first[1].arrive()
        streams[0][1].start(0)
    with scope("first1"):
        first[2].arrive()
        streams[1][0].start(0)
        first[3].arrive()
        streams[1][1].start(0)
    with scope("tokens"):
        for distance in (1, 3, 2):
            tok_copy(distance, tok_from(distance) + c, {X: around(x + distance, NX)}).wait_recv()
            tok_copy(NX + distance, tok_from(distance) + c, {C: other}).start()
    relay(0, 0)
    with scope("tokens2"):
        tok_copy(0, 2 * x + other, {C: other}).wait_recv()
        for distance in range(1, NX):
            tok_copy(NX + distance, tok_from(distance) + other, {C: other}).wait_recv()
    with scope("scale"):
        squares = jnp.zeros((T, 1), F32)
        for k in range(2 * NX):
            block = xg[k].astype(F32)
            squares = squares + jnp.sum(block * block, axis=1, keepdims=True)
            at = slice(k * (D // (2 * NX)), (k + 1) * (D // (2 * NX)))
            sc[:, at] = (block * ngain[:, at]).astype(BF16)
        inv_rms = lax.rsqrt(squares * (1.0 / D) + EPS)
    relay(1, 0)
    relay(0, 1)
    relay(1, 1)
    relay(0, 2)
    relay(1, 2)
    start(2, 0)
    relay(0, 3)

    with scope("gates"):
        scaled = sc[...]
        forget = (mm(scaled, g0a[...].reshape(D, DK)) * inv_rms).astype(BF16).astype(F32)
        value = (mm(scaled, g0b[...].reshape(D, DK)) * inv_rms).astype(BF16)
        r = rate[...]
        series = r * (1.0 - r / 2 * (1.0 - r / 3 * (1.0 - r / 4 * (1.0 - r / 5 * (1.0 - r / 6)))))
        reach = jnp.where(r < 0.1, series, 1.0 - jnp.exp(-r))
        key = reach * (1.0 / (1.0 + jnp.exp(forget)))
        more = lax.dot_general(
            extra[...],
            jnp.ones((1, DK), F32),
            (((0,), (0,)), ((), ())),
            precision=lax.Precision.HIGHEST,
            preferred_element_type=F32,
        )
        logs = jnp.log1p(-key) + more
        row = lax.broadcasted_iota(jnp.int32, (T, T), 0)
        col = lax.broadcasted_iota(jnp.int32, (T, T), 1)
        lower = jnp.where(row >= col, 1.0, 0.0)
        cum = jnp.dot(lower, logs, precision=lax.Precision.HIGHEST, preferred_element_type=F32)
        last = cum[T - 1 : T, :]
        memory = mm2(key * jnp.exp(last - cum), value, 0, 0).T
        st_out[:, 0:16] = memory.astype(BF16).reshape(NR, 16, DK)
        st_out[:, 16:32] = jnp.broadcast_to(log_rows(last)[None], (NR, 16, DK))

    to_slices = Swap(st_out, st1, Y, y, ss.at[0], sr.at[0])
    over_z = Direct(lambda o: st2.at[o], Z, z, ss.at[1], sr.at[1])
    back = Swap(st3_out, st3, Y, y, ss.at[2], sr.at[2])
    to_slices.start()
    st1[y] = st_out[y]
    relay(1, 3)
    start(3, 0)

    with scope("proj_qp"):
        query = (mm(scaled, g1a[0].reshape(D, DK)) * inv_rms).astype(BF16)
        query = query.astype(F32) * DK ** (-0.5)
        pool = (mm(scaled, g1b[0].reshape(D, DK)) * inv_rms).astype(BF16)
        rows_out[...] = pool[T - 16 :, :]
    shift = pltpu.make_async_remote_copy(
        src_ref=rows_out,
        dst_ref=rows_in,
        send_sem=ps.at[0],
        recv_sem=pr.at[0],
        device_id={Z: after_z, Y: after_y},
        device_id_type=MESH,
    )
    shift.start()
    relay(2, 0)

    with scope("wait_y"):
        to_slices.arrive()
    with scope("chain_y"):
        state, total = jnp.zeros((16, DK), F32), jnp.zeros((1, DK), F32)
        inside, before = [], []
        for k in range(NR):
            inside.append(state)
            before.append(total)
            new_state, new_total = from_message(st1, k)
            state = jnp.exp(new_total) * state + new_state
            total = total + new_total
        st2[z] = jnp.concatenate([state.astype(BF16), log_rows(total)], axis=0)
    over_z.start()
    relay(3, 0)

    with scope("diag"):
        value32 = value.astype(F32)
        in_block = lax.rem(lax.broadcasted_iota(jnp.int32, (T, 1), 0), 8)
        decay = jnp.exp(logs)
        weight = query
        rec = jnp.sum(query * key, axis=1, keepdims=True) * value32
        for d in range(1, 8):
            weight = weight * (decay if d == 1 else pltpu.roll(decay, d - 1, 0))
            score = jnp.sum(weight * pltpu.roll(key, d, 0), axis=1, keepdims=True)
            rec = rec + jnp.where(in_block >= d, score, 0.0) * pltpu.roll(value32, d, 0)
    relay(2, 1)
    with scope("wait_z"):
        over_z.arrive()
    with scope("chain_z"):
        state = jnp.zeros((16, DK), F32)
        outer = state
        for k in range(NR):
            new_state, new_total = from_message(st2, k)
            state = jnp.exp(new_total) * state + new_state
            outer = jnp.where(k < z, state, outer)
        for k in range(NR):
            st3_out[k] = (jnp.exp(before[k]) * outer + inside[k]).astype(BF16)
    back.start()
    st3[y] = st3_out[y]
    relay(3, 1)
    with scope("levels"):
        scores = jnp.zeros((T, T), F32)
        for half in (8, 16, 32, 64, 128):
            apart = cum.reshape(T // (2 * half), 2 * half, DK)
            apart = jnp.abs(apart - apart[:, half - 1 : half, :]).reshape(T, DK)
            fade = jnp.exp(-apart)
            level = mm3(query * fade, key * fade, 1, 1)
            mask = (row // (2 * half) == col // (2 * half)) & (row // half > col // half)
            scores = jnp.where(mask, level, scores)
        rec = rec + mm2(scores, value)
    relay(2, 2)
    with scope("pool"):
        shift.wait_recv()
        at_start = (z == 0) & (y == 0)
        earlier = jnp.where(at_start, 0.0, rows_in[...].astype(F32))
        pool32 = pool.astype(F32)
        two = jnp.concatenate([earlier, pool32], axis=0)
        two = two + pltpu.roll(two, 1, 0)
        four = two + pltpu.roll(two, 2, 0)
        eight = four + pltpu.roll(four, 4, 0)
        sixteen = eight + pltpu.roll(eight, 8, 0)
        kind = lax.rem(tp, 4)
        sums = jnp.where(kind == 2, eight, sixteen)
        sums = jnp.where(kind == 0, two, jnp.where(kind == 1, four, sums))
        width = jnp.where(kind == 0, 2, jnp.where(kind == 1, 4, jnp.where(kind == 2, 8, 16)))
        place = (z * NR + y) * T + lax.broadcasted_iota(jnp.int32, (T, 1), 0)
        count = jnp.minimum(place + 1, width).astype(F32)
        mixed = (sums[16:] / count - pool32).astype(BF16)
        mapped = mm(mixed, pmix[...]) * pgain[...]
        faded = query * jnp.exp(cum)
    relay(3, 2)
    relay(2, 3)
    with scope("proj_rg"):
        rgate = (mm(scaled, g1a[1].reshape(D, DK)) * inv_rms).astype(BF16).astype(F32)
        pgate = (mm(scaled, g1b[1].reshape(D, DK)) * inv_rms).astype(BF16).astype(F32)
        y_pool = (mapped * silu(pgate)).astype(BF16)
        gate = sgain[...] * silu(rgate)
    relay(3, 3)
    with scope("wait_back"):
        back.arrive()
    with scope("rec"):
        rec = rec + mm2(faded, st3[...].reshape(DK, DK), 1, 1)
        normed = rec * lax.rsqrt(jnp.mean(rec * rec, axis=1, keepdims=True) + EPS)
        y_rec = (normed * gate).astype(BF16)
        yb[...] = jnp.concatenate([y_rec, y_pool], axis=1).reshape(NX, 2, OWN, 2 * DK)

    half_d = D // 2

    def project(parity, side):
        left = yb[:, parity].reshape(NX * OWN, 2 * DK)
        at = slice(side * (NR // 2), (side + 1) * (NR // 2))
        return mm(left[:, :DK], g1a[2, at].reshape(half_d, DK), 1, 1) + mm(
            left[:, DK:], g1b[2, at].reshape(half_d, DK), 1, 1
        )

    def sib_copy(side):
        return pltpu.make_async_remote_copy(
            src_ref=sib_out.at[side],
            dst_ref=sib_in.at[side],
            send_sem=bs.at[side],
            recv_sem=br.at[side],
            device_id={C: other},
            device_id_type=MESH,
        )

    def red_copy(at, src, dst, step):
        return pltpu.make_async_remote_copy(
            src_ref=src,
            dst_ref=dst,
            send_sem=xs.at[at],
            recv_sem=xr.at[at],
            device_id={X: around(x + step, NX)},
            device_id_type=MESH,
        )

    right, left, across = around(x + 1, NX), around(x - 1, NX), around(x + 2, NX)
    steps = (1, -1)
    over = [red_copy(k, red_out.at[k, across], mid_in.at[k], steps[k]) for k in range(2)]
    near = [red_copy(2 + k, red_out.at[1 - k, (right, left)[k]], red_in.at[k], steps[k]) for k in range(2)]
    merged = [red_copy(4 + k, red_out.at[k, (right, left)[k]], red_in.at[2 + k], steps[k]) for k in range(2)]
    with scope("proj_sib"):
        for side in range(2):
            sib_out[side] = project(other, side).astype(BF16).reshape(NX, OWN, half_d)
            sib_copy(side).start()
    with scope("proj_mine"):
        for side in range(2):
            part = project(c, side).reshape(NX, OWN, half_d)
            sib_copy(side).wait_recv()
            red_out[side] = (part + sib_in[side].astype(F32)).astype(BF16)
            over[side].start()
        for k in range(2):
            near[k].start()
    with scope("red_mid"):
        for k in range(2):
            over[k].wait_recv()
            place = (right, left)[k]
            red_out[k, place] = (red_out[k, place].astype(F32) + mid_in[k].astype(F32)).astype(BF16)
            merged[k].start()
    with scope("red_wait"):
        for k in range(2):
            near[k].wait_recv()
        for k in range(2):
            merged[k].wait_recv()
    with scope("final"):
        low = red_out[0, x].astype(F32) + red_in[2].astype(F32) + red_in[1].astype(F32)
        high = red_out[1, x].astype(F32) + red_in[0].astype(F32) + red_in[3].astype(F32)
        squares = jnp.sum(low * low, axis=1, keepdims=True) + jnp.sum(high * high, axis=1, keepdims=True)
        scale = lax.rsqrt(squares * (1.0 / D) + EPS)
        out[:, :half_d] = (low * scale * post[:, :half_d]).astype(BF16)
        out[:, half_d:] = (high * scale * post[:, half_d:]).astype(BF16)

    with scope("drain"):
        for stream in first + [ring for pair in streams for ring in pair] + [to_slices, over_z, back]:
            stream.drain()
        for distance in range(1, NX):
            tok_out(distance).wait_send()
            tok_copy(NX + distance, tok_from(distance) + c, {C: other}).wait_send()
        tok_copy(0, tp, {C: other}).wait_send()
        for k in range(2):
            sib_copy(k).wait_send()
        for copy in over + near + merged:
            copy.wait_send()
        shift.wait_send()


def per_device(
    tokens_in, norm_gain, w_query, w_forget, w_input, w_rgate, w_pool_in, w_pgate,
    floor_rate, extra_logdecay, state_gain, pool_mix, pool_gain, out_rec, out_pool, post_gain,
):
    anywhere = pl.BlockSpec(memory_space=pl.ANY)
    dma = pltpu.SemaphoreType.DMA
    rows = D // 64
    return pl.pallas_call(
        layer,
        name="layer",
        out_shape=jax.ShapeDtypeStruct((OWN, D), BF16),
        in_specs=[anywhere] * 16,
        out_specs=pl.BlockSpec(memory_space=pltpu.VMEM),
        scratch_shapes=[
            pltpu.VMEM((NR, NR, rows, DK), BF16),
            pltpu.VMEM((NR, NR, rows, DK), BF16),
            pltpu.VMEM((3, NR, NR, rows, DK), BF16),
            pltpu.VMEM((3, NR, NR, rows, DK), BF16),
            pltpu.VMEM((2 * NX, T, D // (2 * NX)), BF16),
            pltpu.VMEM((T, D), BF16),
            pltpu.VMEM((1, D), F32),
            pltpu.VMEM((1, DK), F32),
            pltpu.VMEM((1, T), F32),
            pltpu.VMEM((1, DK), F32),
            pltpu.VMEM((DK, DK), BF16),
            pltpu.VMEM((1, DK), F32),
            pltpu.VMEM((1, D), F32),
            pltpu.VMEM((NR, 32, DK), BF16),
            pltpu.VMEM((NR, 32, DK), BF16),
            pltpu.VMEM((NR, 32, DK), BF16),
            pltpu.VMEM((NR, 16, DK), BF16),
            pltpu.VMEM((NR, 16, DK), BF16),
            pltpu.VMEM((16, DK), BF16),
            pltpu.VMEM((16, DK), BF16),
            pltpu.VMEM((NX, 2, OWN, 2 * DK), BF16),
            pltpu.VMEM((2, NX, OWN, D // 2), BF16),
            pltpu.VMEM((2, NX, OWN, D // 2), BF16),
            pltpu.VMEM((2, NX, OWN, D // 2), BF16),
            pltpu.VMEM((4, OWN, D // 2), BF16),
            pltpu.VMEM((2, OWN, D // 2), BF16),
            dma((9,)),
            dma((7,)),
            dma((4, NR)),
            dma((4, NR)),
            dma((8, NR)),
            dma((8, NR)),
            dma((2 * NX,)),
            dma((2 * NX,)),
            dma((3, NR)),
            dma((3, NR)),
            dma((1,)),
            dma((1,)),
            dma((2,)),
            dma((2,)),
            dma((6,)),
            dma((6,)),
        ],
        compiler_params=pltpu.CompilerParams(
            collective_id=0, has_side_effects=True, vmem_limit_bytes=60 * 1024 * 1024
        ),
    )(
        tokens_in,
        w_query,
        w_forget,
        w_input,
        w_rgate,
        w_pool_in,
        w_pgate,
        out_rec.T,
        out_pool.T,
        norm_gain.reshape(1, -1),
        floor_rate.reshape(1, -1),
        extra_logdecay.reshape(1, -1),
        state_gain.reshape(1, -1),
        pool_mix.reshape(DK, DK),
        pool_gain.reshape(1, -1),
        post_gain.reshape(1, -1),
    )


def solution(mesh):
    torus = Mesh(mesh.devices.reshape(8, 8, 4, 2), ("sp_0", "sp_1", "tp_0", "tp_1"))
    return jax.shard_map(
        per_device,
        mesh=torus,
        in_specs=(
            P(SP, TP),
            P(),
            P(SP, TP),
            P(SP, TP),
            P(SP, TP),
            P(SP, TP),
            P(SP, TP),
            P(SP, TP),
            P(TP),
            P(SP, TP),
            P(TP),
            P(TP, None, None),
            P(TP),
            P(TP, SP),
            P(TP, SP),
            P(),
        ),
        out_specs=P(SP_TP, None),
        check_vma=False,
    )
```

time: 78.3 us -> 73.6 us (0.940)
  Pallas kernels: 76.5 us -> 71.9 us
    pallas_call x1, Pallas kernels: 76.5 us -> 71.9 us  [per_device(): pl.pallas_call(layer, name='layer', out_shape=jax.ShapeDtypeStruct((OWN,...]
where the time goes in v2:
time: 73.6 us; the launch traced here: 73.5 us
  Pallas kernels  71.9 us (98%)
  local copies, waits for them, and re-layouts  1.57 us (2%)
    pallas_call x1, Pallas kernels, per_device(): pl.pallas_call(layer, name='layer', out_shape=jax.ShapeDtypeStruct((OWN,...  71.9 us
    unnamed x1, local copies, waits for them, and re-layouts  1.57 us

profile of v2, /device:TPU:1, one launch (start us, length us, event | category | flops | bytes accessed | tf_op | source)
XLA Modules:
  0.0 73.5 jit_solution(17681311016416739809)
XLA Ops:
  0.0 71.9 %layer.1 = bf16[32,2048]{1,0:T(8,128)(2,1)} custom-call(bf16[256,256]{1,0:T(8,128)(2,1)} %tok.1, bf16[32,128]{1,0:T(8,128)(2,1)} %wq.1, bf16[32,128]{1,0:T(8,128)(2,1)} %wf.1, bf16[32,128]{1,0:T(8,128)(2,1)} %wi.1, bf16[32,128]{1,0:T(8,128)(2,1)} %wr.1, bf16[32,128]{1,0:T(8,128)(2,1)} %wp.1, bf16[32,128]{1,0:T(8,128)(2,1)} %wg.1, bf16[32,128]{1,0:T(8,128)(2,1)} %bitcast.10, ...), custom_call_target="tpu_custom_call" | custom-call | tf_op jit(solution)/shard_map/layer/pallas_call | solution.py:550
  71.9 1.6 %copy.18 = bf16[32,2048]{1,0:T(8,128)(2,1)} copy(bf16[32,2048]{1,0:T(8,128)(2,1)} %layer.1) | data formatting | bytes 262144

commit v3 on v2

--- a/solution.py
+++ b/solution.py
@@ -22,6 +22,8 @@
 OWN = T // (2 * NX)
 F32 = jnp.float32
 BF16 = jnp.bfloat16
+CUTS = 2
+SPAN = NR // CUTS
 ORDER = (4, 3, 5, 2, 6, 1, 7)
 
 
@@ -57,10 +59,10 @@
     def __init__(self, part, axis, me, sign, send, recv):
         self.part, self.axis, self.me, self.sign, self.send, self.recv = part, axis, me, sign, send, recv
 
-    def copy(self, step, back, origin):
+    def copy(self, step, back, cut, origin):
         sign = -self.sign if back else self.sign
-        at = NR // 2 + step if back else step
-        block = self.part(origin)
+        at = CUTS * (NR // 2 + step if back else step) + cut
+        block = self.part(origin, cut)
         return pltpu.make_async_remote_copy(
             src_ref=block,
             dst_ref=block,
@@ -77,20 +79,20 @@
     def steps(self, back):
         return NR // 2 - 1 if back else NR // 2
 
-    def start(self, step):
-        for back in (False, True):
-            if step < self.steps(back):
-                self.copy(step, back, self.origin(step, back)).start()
-
-    def arrive(self, step):
-        for back in (False, True):
-            if step < self.steps(back):
-                self.copy(step, back, self.origin(step + 1, back)).wait_recv()
+    def start(self, step, back, cut):
+        if step < self.steps(back):
+            self.copy(step, back, cut, self.origin(step, back)).start()
+
+    def relay(self, step, back, cut):
+        if step < self.steps(back):
+            self.copy(step, back, cut, self.origin(step + 1, back)).wait_recv()
+            self.start(step + 1, back, cut)
 
     def drain(self):
         for back in (False, True):
             for step in range(self.steps(back)):
-                self.copy(step, back, self.origin(step, back)).wait_send()
+                for cut in range(CUTS):
+                    self.copy(step, back, cut, self.origin(step, back)).wait_send()
 
 
 class Direct:
@@ -179,6 +181,20 @@
     sign = 1 - 2 * c
     other = 1 - c
 
+    after_y = around(y + 1, NR)
+    after_z = jnp.where(y == NR - 1, around(z + 1, NR), z)
+    before_y = around(y - 1, NR)
+    before_z = jnp.where(y == 0, around(z - 1, NR), z)
+    with scope("barrier"):
+        barrier = pltpu.get_barrier_semaphore()
+        for k in ORDER:
+            pl.semaphore_signal(barrier, 1, device_id={Y: around(y + k, NR)}, device_id_type=MESH)
+            pl.semaphore_signal(barrier, 1, device_id={Z: around(z + k, NR)}, device_id_type=MESH)
+        for k in range(1, NX):
+            pl.semaphore_signal(barrier, 1, device_id={X: around(x + k, NX)}, device_id_type=MESH)
+        pl.semaphore_signal(barrier, 1, device_id={C: other}, device_id_type=MESH)
+        pl.semaphore_signal(barrier, 1, device_id={Z: before_z, Y: before_y}, device_id_type=MESH)
+
     local = [
         pltpu.make_async_copy(src, dst, lsem.at[k])
         for k, (src, dst) in enumerate(
@@ -211,51 +227,52 @@
     ]
     for copy in local + vectors:
         copy.start()
-
-    after_y = around(y + 1, NR)
-    after_z = jnp.where(y == NR - 1, around(z + 1, NR), z)
-    before_y = around(y - 1, NR)
-    before_z = jnp.where(y == 0, around(z - 1, NR), z)
     with scope("barrier"):
-        barrier = pltpu.get_barrier_semaphore()
-        for k in ORDER:
-            pl.semaphore_signal(barrier, 1, device_id={Y: around(y + k, NR)}, device_id_type=MESH)
-            pl.semaphore_signal(barrier, 1, device_id={Z: around(z + k, NR)}, device_id_type=MESH)
-        for k in range(1, NX):
-            pl.semaphore_signal(barrier, 1, device_id={X: around(x + k, NX)}, device_id_type=MESH)
-        pl.semaphore_signal(barrier, 1, device_id={C: other}, device_id_type=MESH)
-        pl.semaphore_signal(barrier, 1, device_id={Z: before_z, Y: before_y}, device_id_type=MESH)
         pl.semaphore_wait(barrier, 2 * (NR - 1) + NX - 1 + 2)
 
     first = [
-        Direct(lambda o: g0a.at[z, o], Y, y, p1s.at[0], p1r.at[0]),
-        Direct(lambda o: g0b.at[o, y], Z, z, p1s.at[1], p1r.at[1]),
-        Direct(lambda o: g1a.at[:, z, o], Y, y, p1s.at[2], p1r.at[2]),
-        Direct(lambda o: g1b.at[:, o, y], Z, z, p1s.at[3], p1r.at[3]),
+        (
+            Direct(lambda o: g0a.at[z, o], Y, y, p1s.at[0], p1r.at[0]),
+            Direct(lambda o: g0b.at[o, y], Z, z, p1s.at[1], p1r.at[1]),
+        )
+    ] + [
+        (
+            Direct(lambda o, k=k: g1a.at[k, z, o], Y, y, p1s.at[2 * k + 2], p1r.at[2 * k + 2]),
+            Direct(lambda o, k=k: g1b.at[k, o, y], Z, z, p1s.at[2 * k + 3], p1r.at[2 * k + 3]),
+        )
+        for k in range(3)
     ]
+
+    def cut_of(cut):
+        return pl.ds(SPAN * cut, SPAN)
+
     streams = [
         (
-            Ring(lambda o: g0a.at[o], Z, z, sign, p2s.at[0], p2r.at[0]),
-            Ring(lambda o: g0b.at[:, o], Y, y, sign, p2s.at[1], p2r.at[1]),
+            Ring(lambda o, u: g0a.at[o, cut_of(u)], Z, z, sign, p2s.at[0], p2r.at[0]),
+            Ring(lambda o, u: g0b.at[cut_of(u), o], Y, y, sign, p2s.at[1], p2r.at[1]),
         )
     ] + [
         (
-            Ring(lambda o, k=k: g1a.at[k, o], Z, z, sign, p2s.at[2 * k + 2], p2r.at[2 * k + 2]),
-            Ring(lambda o, k=k: g1b.at[k, :, o], Y, y, sign, p2s.at[2 * k + 3], p2r.at[2 * k + 3]),
+            Ring(lambda o, u, k=k: g1a.at[k, o, cut_of(u)], Z, z, sign, p2s.at[2 * k + 2], p2r.at[2 * k + 2]),
+            Ring(lambda o, u, k=k: g1b.at[k, cut_of(u), o], Y, y, sign, p2s.at[2 * k + 3], p2r.at[2 * k + 3]),
         )
         for k in range(3)
     ]
 
-    def start(k, step):
-        for ring in streams[k]:
-            ring.start(step)
+    def start(k):
+        with scope("first%d" % k):
+            for wide, ring in zip(first[k], streams[k]):
+                wide.arrive()
+                for cut in range(CUTS):
+                    for back in (False, True):
+                        ring.start(0, back, cut)
 
     def relay(k, step):
         with scope("relay%d%d" % (k, step)):
-            for ring in streams[k]:
-                ring.arrive(step)
-                if step + 1 < NR // 2:
-                    ring.start(step + 1)
+            for cut in range(CUTS):
+                for back in (False, True):
+                    for ring in streams[k]:
+                        ring.relay(step, back, cut)
 
     def tok_copy(at, slot, where):
         return pltpu.make_async_remote_copy(
@@ -275,32 +292,27 @@
 
     with scope("sends"):
         local[0].wait()
-        first[0].start()
+        first[0][0].start()
         local[1].wait()
-        first[1].start()
+        first[0][1].start()
         local[2].wait()
         for distance in (2, 1, 3):
             tok_out(distance).start()
         tok_copy(0, tp, {C: other}).start()
-        for k in range(3, 6):
-            local[k].wait()
-        first[2].start()
-        for k in range(6, 9):
-            local[k].wait()
-        first[3].start()
+        for k in range(2):
+            local[3 + k].wait()
+            first[1 + k][0].start()
+            local[6 + k].wait()
+            first[1 + k][1].start()
+        local[5].wait()
+        local[8].wait()
         for copy in vectors:
             copy.wait()
 
-    with scope("first0"):
-        first[0].arrive()
-        streams[0][0].start(0)
-        first[1].arrive()
-        streams[0][1].start(0)
-    with scope("first1"):
-        first[2].arrive()
-        streams[1][0].start(0)
-        first[3].arrive()
-        streams[1][1].start(0)
+    start(0)
+    start(1)
+    first[3][0].start()
+    first[3][1].start()
     with scope("tokens"):
         for distance in (1, 3, 2):
             tok_copy(distance, tok_from(distance) + c, {X: around(x + distance, NX)}).wait_recv()
@@ -322,14 +334,17 @@
     relay(0, 1)
     relay(1, 1)
     relay(0, 2)
+    start(2)
     relay(1, 2)
-    start(2, 0)
+    start(3)
     relay(0, 3)
 
-    with scope("gates"):
+    with scope("proj_fv"):
         scaled = sc[...]
         forget = (mm(scaled, g0a[...].reshape(D, DK)) * inv_rms).astype(BF16).astype(F32)
         value = (mm(scaled, g0b[...].reshape(D, DK)) * inv_rms).astype(BF16)
+    relay(2, 0)
+    with scope("gates"):
         r = rate[...]
         series = r * (1.0 - r / 2 * (1.0 - r / 3 * (1.0 - r / 4 * (1.0 - r / 5 * (1.0 - r / 6)))))
         reach = jnp.where(r < 0.1, series, 1.0 - jnp.exp(-r))
@@ -357,7 +372,7 @@
     to_slices.start()
     st1[y] = st_out[y]
     relay(1, 3)
-    start(3, 0)
+    relay(3, 0)
 
     with scope("proj_qp"):
         query = (mm(scaled, g1a[0].reshape(D, DK)) * inv_rms).astype(BF16)
@@ -373,7 +388,7 @@
         device_id_type=MESH,
     )
     shift.start()
-    relay(2, 0)
+    relay(2, 1)
 
     with scope("wait_y"):
         to_slices.arrive()
@@ -388,7 +403,7 @@
             total = total + new_total
         st2[z] = jnp.concatenate([state.astype(BF16), log_rows(total)], axis=0)
     over_z.start()
-    relay(3, 0)
+    relay(3, 1)
 
     with scope("diag"):
         value32 = value.astype(F32)
@@ -400,7 +415,7 @@
             weight = weight * (decay if d == 1 else pltpu.roll(decay, d - 1, 0))
             score = jnp.sum(weight * pltpu.roll(key, d, 0), axis=1, keepdims=True)
             rec = rec + jnp.where(in_block >= d, score, 0.0) * pltpu.roll(value32, d, 0)
-    relay(2, 1)
+    relay(2, 2)
     with scope("wait_z"):
         over_z.arrive()
     with scope("chain_z"):
@@ -414,7 +429,7 @@
             st3_out[k] = (jnp.exp(before[k]) * outer + inside[k]).astype(BF16)
     back.start()
     st3[y] = st3_out[y]
-    relay(3, 1)
+    relay(3, 2)
     with scope("levels"):
         scores = jnp.zeros((T, T), F32)
         for half in (8, 16, 32, 64, 128):
@@ -425,7 +440,6 @@
             mask = (row // (2 * half) == col // (2 * half)) & (row // half > col // half)
             scores = jnp.where(mask, level, scores)
         rec = rec + mm2(scores, value)
-    relay(2, 2)
     with scope("pool"):
         shift.wait_recv()
         at_start = (z == 0) & (y == 0)
@@ -445,7 +459,6 @@
         mixed = (sums[16:] / count - pool32).astype(BF16)
         mapped = mm(mixed, pmix[...]) * pgain[...]
         faded = query * jnp.exp(cum)
-    relay(3, 2)
     relay(2, 3)
     with scope("proj_rg"):
         rgate = (mm(scaled, g1a[1].reshape(D, DK)) * inv_rms).astype(BF16).astype(F32)
@@ -492,9 +505,19 @@
 
     right, left, across = around(x + 1, NX), around(x - 1, NX), around(x + 2, NX)
     steps = (1, -1)
-    over = [red_copy(k, red_out.at[k, across], mid_in.at[k], steps[k]) for k in range(2)]
-    near = [red_copy(2 + k, red_out.at[1 - k, (right, left)[k]], red_in.at[k], steps[k]) for k in range(2)]
-    merged = [red_copy(4 + k, red_out.at[k, (right, left)[k]], red_in.at[2 + k], steps[k]) for k in range(2)]
+    piece = [pl.ds(0, OWN // 2), pl.ds(OWN // 2, OWN // 2)]
+    over = [
+        [red_copy(2 * k + u, red_out.at[k, across, piece[u]], mid_in.at[k, piece[u]], steps[k]) for u in range(2)]
+        for k in range(2)
+    ]
+    near = [red_copy(4 + k, red_out.at[1 - k, (right, left)[k]], red_in.at[k], steps[k]) for k in range(2)]
+    merged = [
+        [
+            red_copy(6 + 2 * k + u, red_out.at[k, (right, left)[k], piece[u]], red_in.at[2 + k, piece[u]], steps[k])
+            for u in range(2)
+        ]
+        for k in range(2)
+    ]
     with scope("proj_sib"):
         for side in range(2):
             sib_out[side] = project(other, side).astype(BF16).reshape(NX, OWN, half_d)
@@ -504,20 +527,25 @@
             part = project(c, side).reshape(NX, OWN, half_d)
             sib_copy(side).wait_recv()
             red_out[side] = (part + sib_in[side].astype(F32)).astype(BF16)
-            over[side].start()
+            for u in range(2):
+                over[side][u].start()
         for k in range(2):
             near[k].start()
     with scope("red_mid"):
-        for k in range(2):
-            over[k].wait_recv()
-            place = (right, left)[k]
-            red_out[k, place] = (red_out[k, place].astype(F32) + mid_in[k].astype(F32)).astype(BF16)
-            merged[k].start()
+        for u in range(2):
+            for k in range(2):
+                over[k][u].wait_recv()
+                place = (right, left)[k]
+                red_out[k, place, piece[u]] = (
+                    red_out[k, place, piece[u]].astype(F32) + mid_in[k, piece[u]].astype(F32)
+                ).astype(BF16)
+                merged[k][u].start()
     with scope("red_wait"):
         for k in range(2):
             near[k].wait_recv()
         for k in range(2):
-            merged[k].wait_recv()
+            for u in range(2):
+                merged[k][u].wait_recv()
     with scope("final"):
         low = red_out[0, x].astype(F32) + red_in[2].astype(F32) + red_in[1].astype(F32)
         high = red_out[1, x].astype(F32) + red_in[0].astype(F32) + red_in[3].astype(F32)
@@ -527,7 +555,7 @@
         out[:, half_d:] = (high * scale * post[:, half_d:]).astype(BF16)
 
     with scope("drain"):
-        for stream in first + [ring for pair in streams for ring in pair] + [to_slices, over_z, back]:
+        for stream in [one for pair in first + streams for one in pair] + [to_slices, over_z, back]:
             stream.drain()
         for distance in range(1, NX):
             tok_out(distance).wait_send()
@@ -535,7 +563,7 @@
         tok_copy(0, tp, {C: other}).wait_send()
         for k in range(2):
             sib_copy(k).wait_send()
-        for copy in over + near + merged:
+        for copy in over[0] + over[1] + near + merged[0] + merged[1]:
             copy.wait_send()
         shift.wait_send()
 
@@ -547,7 +575,7 @@
     anywhere = pl.BlockSpec(memory_space=pl.ANY)
     dma = pltpu.SemaphoreType.DMA
     rows = D // 64
-    return pl.pallas_call(
+    run = pl.pallas_call(
         layer,
         name="layer",
         out_shape=jax.ShapeDtypeStruct((OWN, D), BF16),
@@ -582,10 +610,10 @@
             pltpu.VMEM((2, OWN, D // 2), BF16),
             dma((9,)),
             dma((7,)),
-            dma((4, NR)),
-            dma((4, NR)),
             dma((8, NR)),
             dma((8, NR)),
+            dma((8, CUTS * NR)),
+            dma((8, CUTS * NR)),
             dma((2 * NX,)),
             dma((2 * NX,)),
             dma((3, NR)),
@@ -594,13 +622,14 @@
             dma((1,)),
             dma((2,)),
             dma((2,)),
-            dma((6,)),
-            dma((6,)),
+            dma((10,)),
+            dma((10,)),
         ],
         compiler_params=pltpu.CompilerParams(
-            collective_id=0, has_side_effects=True, vmem_limit_bytes=60 * 1024 * 1024
+            collective_id=0, has_side_effects=True, vmem_limit_bytes=32 * 1024 * 1024
         ),
-    )(
+    )
+    operands = (
         tokens_in,
         w_query,
         w_forget,
@@ -618,6 +647,7 @@
         pool_gain.reshape(1, -1),
         post_gain.reshape(1, -1),
     )
+    return run(*[pltpu.with_memory_space_constraint(a, pltpu.HBM) for a in operands])
 
 
 def solution(mesh):

time: 73.6 us -> 66.6 us (0.905)
  Pallas kernels: 71.9 us -> 65.8 us
  local copies, waits for them, and re-layouts: 1.57 us -> 0.66 us
    pallas_call x1, Pallas kernels: 71.9 us -> 65.8 us  [per_device(): run(*[pltpu.with_memory_space_constraint(a, pltpu.HBM) for a in operands])]
    unnamed x1, local copies, waits for them, and re-layouts: 1.57 us -> 0.66 us
where the time goes in v3:
time: 66.6 us; the launch traced here: 66.5 us
  Pallas kernels  65.8 us (99%)
    pallas_call x1, Pallas kernels, per_device(): run(*[pltpu.with_memory_space_constraint(a, pltpu.HBM) for a in operands])  65.8 us

profile of v3, /device:TPU:1, one launch (start us, length us, event | category | flops | bytes accessed | tf_op | source)
XLA Modules:
  0.0 66.5 jit_solution(7389582942250027153)
XLA Ops:
  0.0 65.8 %layer.1 = bf16[32,2048]{1,0:T(8,128)(2,1)S(1)} custom-call(bf16[256,256]{1,0:T(8,128)(2,1)} %tok.1, bf16[32,128]{1,0:T(8,128)(2,1)} %wq.1, bf16[32,128]{1,0:T(8,128)(2,1)} %wf.1, bf16[32,128]{1,0:T(8,128)(2,1)} %wi.1, bf16[32,128]{1,0:T(8,128)(2,1)} %wr.1, bf16[32,128]{1,0:T(8,128)(2,1)} %wp.1, bf16[32,128]{1,0:T(8,128)(2,1)} %wg.1, ...), custom_call_target="tpu_custom_call" | custom-call | tf_op jit(solution)/shard_map/layer/pallas_call | solution.py:650
  65.9 0.7 copy.18

commit v4 on v3

--- a/solution.py
+++ b/solution.py
@@ -55,100 +55,133 @@
     return lax.rem(value + 2 * count, count)
 
 
-class Ring:
-    def __init__(self, part, axis, me, sign, send, recv):
-        self.part, self.axis, self.me, self.sign, self.send, self.recv = part, axis, me, sign, send, recv
+def remote(src, dst, send, recv, where):
+    return pltpu.make_async_remote_copy(
+        src_ref=src, dst_ref=dst, send_sem=send, recv_sem=recv, device_id=where, device_id_type=MESH
+    )
+
+
+class Stream:
+    def __init__(self, at, wide, long, w, l, sign, sems):
+        self.at, self.wide, self.long, self.w, self.l, self.sign = at, wide, long, w, l, sign
+        self.send1, self.send2, self.recv1, self.recv2 = sems
+
+    def first_copy(self, distance, origin, recv):
+        block = self.at(pl.ds(origin, 1), pl.ds(self.l, 1))
+        return remote(block, block, self.send1, recv, {self.wide: around(self.w + distance, NR)})
+
+    def first_start(self):
+        for distance in ORDER:
+            self.first_copy(distance, self.w, self.recv1).start()
+
+    def first_arrive(self):
+        view = self.at(pl.ds(0, NR - 1), pl.ds(self.l, 1))
+        remote(view, view, self.send1, self.recv1, {self.wide: around(self.w + 1, NR)}).wait_recv()
+
+    def drain(self):
+        view = self.at(pl.ds(0, NR - 1), pl.ds(self.l, 1))
+        remote(view, view, self.send1, self.send1, {self.wide: around(self.w + 1, NR)}).wait_send()
+        view = self.at(pl.ds(0, NR), pl.ds(0, NR - 1))
+        remote(view, view, self.send2, self.send2, {self.long: around(self.l + 1, NR)}).wait_send()
+
+    def origin(self, step, back):
+        sign = -self.sign if back else self.sign
+        return around(self.l - sign * step, NR)
+
+    def steps(self, back):
+        return NR // 2 - 1 if back else NR // 2
+
+    def sem(self, step, back, cut):
+        if step == self.steps(back) - 1:
+            return self.recv2.at[1 if back else 0]
+        return self.recv2.at[2 + CUTS * (NR // 2 - 1 + step if back else step) + cut]
 
     def copy(self, step, back, cut, origin):
         sign = -self.sign if back else self.sign
-        at = CUTS * (NR // 2 + step if back else step) + cut
-        block = self.part(origin, cut)
-        return pltpu.make_async_remote_copy(
-            src_ref=block,
-            dst_ref=block,
-            send_sem=self.send.at[at],
-            recv_sem=self.recv.at[at],
-            device_id={self.axis: around(self.me + sign, NR)},
-            device_id_type=MESH,
-        )
-
-    def origin(self, step, back):
-        sign = -self.sign if back else self.sign
-        return around(self.me - sign * step, NR)
-
-    def steps(self, back):
-        return NR // 2 - 1 if back else NR // 2
+        block = self.at(pl.ds(SPAN * cut, SPAN), pl.ds(origin, 1))
+        where = {self.long: around(self.l + sign, NR)}
+        return remote(block, block, self.send2, self.sem(step, back, cut), where)
 
     def start(self, step, back, cut):
         if step < self.steps(back):
             self.copy(step, back, cut, self.origin(step, back)).start()
 
     def relay(self, step, back, cut):
-        if step < self.steps(back):
+        if step < self.steps(back) - 1:
             self.copy(step, back, cut, self.origin(step + 1, back)).wait_recv()
             self.start(step + 1, back, cut)
-
-    def drain(self):
-        for back in (False, True):
-            for step in range(self.steps(back)):
-                for cut in range(CUTS):
-                    self.copy(step, back, cut, self.origin(step, back)).wait_send()
+        elif step == self.steps(back) - 1 and cut == CUTS - 1:
+            block = self.at(pl.ds(0, NR), pl.ds(self.origin(step + 1, back), 1))
+            where = {self.long: around(self.l + self.sign, NR)}
+            remote(block, block, self.send2, self.sem(step, back, cut), where).wait_recv()
+
+
+class FastStream(Stream):
+    def first_start(self):
+        pair, twin = self.w // 2, self.w + 1 - 2 * lax.rem(self.w, 2)
+        for ahead in (2, 1, 3):
+            for k in range(2):
+                place = 2 * lax.rem(pair + ahead, NR // 2) + k
+                block = self.at(pl.ds(self.w, 1), pl.ds(self.l, 1))
+                remote(block, block, self.send1, self.recv1.at[NR // 2 - ahead], {self.wide: place}).start()
+        block = self.at(pl.ds(self.w, 1), pl.ds(self.l, 1))
+        remote(block, block, self.send1, self.recv1.at[0], {self.wide: twin}).start()
+
+    def pair_at(self, ahead):
+        return 2 * lax.rem(self.w // 2 + ahead, NR // 2)
+
+    def first_arrive(self, ahead):
+        twin = self.w + 1 - 2 * lax.rem(self.w, 2)
+        if ahead == 0:
+            view = self.at(pl.ds(twin, 1), pl.ds(self.l, 1))
+        else:
+            view = self.at(pl.ds(self.pair_at(ahead), 2), pl.ds(self.l, 1))
+        remote(view, view, self.send1, self.recv1.at[ahead], {self.wide: twin}).wait_recv()
+
+    def hop(self, ahead, origin, move, sem):
+        block = self.at(pl.ds(self.pair_at(ahead), 2), pl.ds(origin, 1))
+        where = {self.long: around(self.l + self.sign * move, NR)}
+        return remote(block, block, self.send2, self.recv2.at[sem], where)
+
+    def send_own(self, ahead):
+        for move, sem in ((2, 5 + ahead), (-2, 9 + ahead), (1, 0), (-1, 3)):
+            self.hop(ahead, self.l, move, sem).start()
+
+    def send_on(self, ahead):
+        origin = around(self.l - 2 * self.sign, NR)
+        self.hop(ahead, origin, 2, 5 + ahead).wait_recv()
+        self.hop(ahead, origin, 2, 2).start()
+        self.hop(ahead, origin, 1, 1).start()
+        origin = around(self.l + 2 * self.sign, NR)
+        self.hop(ahead, origin, -2, 9 + ahead).wait_recv()
+        self.hop(ahead, origin, -1, 4).start()
+
+    def finish(self):
+        for move, sem in ((1, 0), (-1, 3), (3, 1), (-3, 4), (4, 2)):
+            block = self.at(pl.ds(0, NR), pl.ds(around(self.l - self.sign * move, NR), 1))
+            where = {self.long: around(self.l + self.sign, NR)}
+            remote(block, block, self.send2, self.recv2.at[sem], where).wait_recv()
 
 
 class Direct:
-    def __init__(self, part, axis, me, send, recv):
-        self.part, self.axis, self.me, self.send, self.recv = part, axis, me, send, recv
-
-    def copy(self, distance, origin):
-        block = self.part(origin)
-        return pltpu.make_async_remote_copy(
-            src_ref=block,
-            dst_ref=block,
-            send_sem=self.send.at[distance],
-            recv_sem=self.recv.at[distance],
-            device_id={self.axis: around(self.me + distance, NR)},
-            device_id_type=MESH,
-        )
+    def __init__(self, held, axis, me, send, recv, out=None):
+        self.out, self.held, self.axis, self.me, self.send, self.recv = out, held, axis, me, send, recv
 
     def start(self):
         for distance in ORDER:
-            self.copy(distance, self.me).start()
+            place = around(self.me + distance, NR)
+            src = self.held.at[self.me] if self.out is None else self.out.at[place]
+            remote(src, self.held.at[self.me], self.send, self.recv, {self.axis: place}).start()
+
+    def whole(self):
+        view = self.held.at[pl.ds(0, NR - 1)]
+        return remote(view, view, self.send, self.recv, {self.axis: around(self.me + 1, NR)})
 
     def arrive(self):
-        for distance in range(1, NR):
-            self.copy(distance, around(self.me - distance, NR)).wait_recv()
+        self.whole().wait_recv()
 
     def drain(self):
-        for distance in range(1, NR):
-            self.copy(distance, self.me).wait_send()
-
-
-class Swap:
-    def __init__(self, out, held, axis, me, send, recv):
-        self.out, self.held, self.axis, self.me, self.send, self.recv = out, held, axis, me, send, recv
-
-    def copy(self, distance, origin):
-        other = around(self.me + distance, NR)
-        return pltpu.make_async_remote_copy(
-            src_ref=self.out.at[other],
-            dst_ref=self.held.at[origin],
-            send_sem=self.send.at[distance],
-            recv_sem=self.recv.at[distance],
-            device_id={self.axis: other},
-            device_id_type=MESH,
-        )
-
-    def start(self):
-        for distance in ORDER:
-            self.copy(distance, self.me).start()
-
-    def arrive(self):
-        for distance in range(1, NR):
-            self.copy(distance, around(self.me - distance, NR)).wait_recv()
-
-    def drain(self):
-        for distance in range(1, NR):
-            self.copy(distance, self.me).wait_send()
+        self.whole().wait_send()
 
 
 def log_rows(total):
@@ -173,7 +206,7 @@
     g0a, g0b, g1a, g1b, xg, sc,
     ngain, rate, extra, sgain, pmix, pgain, post,
     st_out, st1, st2, st3_out, st3, rows_out, rows_in, yb, sib_out, sib_in, red_out, red_in, mid_in,
-    lsem, vsem, p1s, p1r, p2s, p2r, ts, tr, ss, sr, ps, pr, bs, br, xs, xr,
+    lsem, vsem, f1r, f2r, p1s, p1r, p2s, p2r, ts, tr, ss, sr, ps, pr, bs, br, xs, xr,
 ):
     scope = jax.named_scope
     z, y, x, c = lax.axis_index(Z), lax.axis_index(Y), lax.axis_index(X), lax.axis_index(C)
@@ -230,98 +263,85 @@
     with scope("barrier"):
         pl.semaphore_wait(barrier, 2 * (NR - 1) + NX - 1 + 2)
 
-    first = [
-        (
-            Direct(lambda o: g0a.at[z, o], Y, y, p1s.at[0], p1r.at[0]),
-            Direct(lambda o: g0b.at[o, y], Z, z, p1s.at[1], p1r.at[1]),
-        )
-    ] + [
-        (
-            Direct(lambda o, k=k: g1a.at[k, z, o], Y, y, p1s.at[2 * k + 2], p1r.at[2 * k + 2]),
-            Direct(lambda o, k=k: g1b.at[k, o, y], Z, z, p1s.at[2 * k + 3], p1r.at[2 * k + 3]),
-        )
+    def stream(kind, buffer, flip, at, recv1, recv2):
+        sems = (p1s.at[at], p2s.at[at], recv1, recv2)
+        if flip:
+            return kind(lambda w, l: buffer.at[w, l], Z, Y, z, y, sign, sems)
+        return kind(lambda w, l: buffer.at[l, w], Y, Z, y, z, sign, sems)
+
+    fast = [
+        stream(FastStream, buffer, flip, flip, f1r.at[flip], f2r.at[flip])
+        for flip, buffer in enumerate((g0a, g0b))
+    ]
+    streams = [
+        [
+            stream(Stream, buffer.at[k], flip, 2 * k + 2 + flip, p1r.at[2 * k + flip], p2r.at[2 * k + flip])
+            for flip, buffer in enumerate((g1a, g1b))
+        ]
         for k in range(3)
     ]
-
-    def cut_of(cut):
-        return pl.ds(SPAN * cut, SPAN)
-
-    streams = [
-        (
-            Ring(lambda o, u: g0a.at[o, cut_of(u)], Z, z, sign, p2s.at[0], p2r.at[0]),
-            Ring(lambda o, u: g0b.at[cut_of(u), o], Y, y, sign, p2s.at[1], p2r.at[1]),
-        )
-    ] + [
-        (
-            Ring(lambda o, u, k=k: g1a.at[k, o, cut_of(u)], Z, z, sign, p2s.at[2 * k + 2], p2r.at[2 * k + 2]),
-            Ring(lambda o, u, k=k: g1b.at[k, cut_of(u), o], Y, y, sign, p2s.at[2 * k + 3], p2r.at[2 * k + 3]),
-        )
-        for k in range(3)
-    ]
+    streams = [fast] + streams
 
     def start(k):
         with scope("first%d" % k):
-            for wide, ring in zip(first[k], streams[k]):
-                wide.arrive()
+            for one in streams[k]:
+                one.first_arrive()
                 for cut in range(CUTS):
                     for back in (False, True):
-                        ring.start(0, back, cut)
+                        one.start(0, back, cut)
 
     def relay(k, step):
         with scope("relay%d%d" % (k, step)):
             for cut in range(CUTS):
                 for back in (False, True):
-                    for ring in streams[k]:
-                        ring.relay(step, back, cut)
+                    for one in streams[k]:
+                        one.relay(step, back, cut)
+
+    def first_start(k):
+        for one in streams[k]:
+            one.first_start()
 
     def tok_copy(at, slot, where):
-        return pltpu.make_async_remote_copy(
-            src_ref=xg.at[slot],
-            dst_ref=xg.at[slot],
-            send_sem=ts.at[at],
-            recv_sem=tr.at[at],
-            device_id=where,
-            device_id_type=MESH,
-        )
-
-    def tok_out(distance):
-        return tok_copy(distance, tp, {X: around(x + distance, NX)})
+        return remote(xg.at[slot], xg.at[slot], ts.at[0], tr.at[at], where)
 
     def tok_from(distance):
         return 2 * around(x - distance, NX)
 
     with scope("sends"):
         local[0].wait()
-        first[0][0].start()
+        fast[0].first_start()
         local[1].wait()
-        first[0][1].start()
+        fast[1].first_start()
         local[2].wait()
         for distance in (2, 1, 3):
-            tok_out(distance).start()
+            tok_copy(distance, tp, {X: around(x + distance, NX)}).start()
         tok_copy(0, tp, {C: other}).start()
-        for k in range(2):
-            local[3 + k].wait()
-            first[1 + k][0].start()
-            local[6 + k].wait()
-            first[1 + k][1].start()
-        local[5].wait()
-        local[8].wait()
+        for k in range(3, 9):
+            local[k].wait()
+        first_start(1)
+        first_start(2)
         for copy in vectors:
             copy.wait()
 
-    start(0)
-    start(1)
-    first[3][0].start()
-    first[3][1].start()
+    for ahead in (0, 1, 3, 2):
+        with scope("own%d" % ahead):
+            for one in fast:
+                one.first_arrive(ahead)
+                one.send_own(ahead)
     with scope("tokens"):
         for distance in (1, 3, 2):
             tok_copy(distance, tok_from(distance) + c, {X: around(x + distance, NX)}).wait_recv()
-            tok_copy(NX + distance, tok_from(distance) + c, {C: other}).start()
-    relay(0, 0)
+            tok_copy(0, tok_from(distance) + c, {C: other}).start()
+    for ahead in (0, 1, 3, 2):
+        with scope("on%d" % ahead):
+            for one in fast:
+                one.send_on(ahead)
+    start(1)
+    first_start(3)
+    start(2)
     with scope("tokens2"):
-        tok_copy(0, 2 * x + other, {C: other}).wait_recv()
-        for distance in range(1, NX):
-            tok_copy(NX + distance, tok_from(distance) + other, {C: other}).wait_recv()
+        four = xg.at[pl.ds(0, NX)]
+        remote(four, four, ts.at[0], tr.at[0], {C: other}).wait_recv()
     with scope("scale"):
         squares = jnp.zeros((T, 1), F32)
         for k in range(2 * NX):
@@ -330,20 +350,15 @@
             at = slice(k * (D // (2 * NX)), (k + 1) * (D // (2 * NX)))
             sc[:, at] = (block * ngain[:, at]).astype(BF16)
         inv_rms = lax.rsqrt(squares * (1.0 / D) + EPS)
-    relay(1, 0)
-    relay(0, 1)
-    relay(1, 1)
-    relay(0, 2)
-    start(2)
-    relay(1, 2)
-    start(3)
-    relay(0, 3)
+    with scope("finish"):
+        for one in fast:
+            one.finish()
 
     with scope("proj_fv"):
         scaled = sc[...]
         forget = (mm(scaled, g0a[...].reshape(D, DK)) * inv_rms).astype(BF16).astype(F32)
         value = (mm(scaled, g0b[...].reshape(D, DK)) * inv_rms).astype(BF16)
-    relay(2, 0)
+    relay(1, 0)
     with scope("gates"):
         r = rate[...]
         series = r * (1.0 - r / 2 * (1.0 - r / 3 * (1.0 - r / 4 * (1.0 - r / 5 * (1.0 - r / 6)))))
@@ -366,30 +381,16 @@
         st_out[:, 0:16] = memory.astype(BF16).reshape(NR, 16, DK)
         st_out[:, 16:32] = jnp.broadcast_to(log_rows(last)[None], (NR, 16, DK))
 
-    to_slices = Swap(st_out, st1, Y, y, ss.at[0], sr.at[0])
-    over_z = Direct(lambda o: st2.at[o], Z, z, ss.at[1], sr.at[1])
-    back = Swap(st3_out, st3, Y, y, ss.at[2], sr.at[2])
+    to_slices = Direct(st1, Y, y, ss.at[0], sr.at[0], st_out)
+    over_z = Direct(st2, Z, z, ss.at[1], sr.at[1])
+    back = Direct(st3, Y, y, ss.at[2], sr.at[2], st3_out)
     to_slices.start()
     st1[y] = st_out[y]
-    relay(1, 3)
+    relay(2, 0)
+    start(3)
+    relay(1, 1)
+    relay(2, 1)
     relay(3, 0)
-
-    with scope("proj_qp"):
-        query = (mm(scaled, g1a[0].reshape(D, DK)) * inv_rms).astype(BF16)
-        query = query.astype(F32) * DK ** (-0.5)
-        pool = (mm(scaled, g1b[0].reshape(D, DK)) * inv_rms).astype(BF16)
-        rows_out[...] = pool[T - 16 :, :]
-    shift = pltpu.make_async_remote_copy(
-        src_ref=rows_out,
-        dst_ref=rows_in,
-        send_sem=ps.at[0],
-        recv_sem=pr.at[0],
-        device_id={Z: after_z, Y: after_y},
-        device_id_type=MESH,
-    )
-    shift.start()
-    relay(2, 1)
-
     with scope("wait_y"):
         to_slices.arrive()
     with scope("chain_y"):
@@ -403,19 +404,11 @@
             total = total + new_total
         st2[z] = jnp.concatenate([state.astype(BF16), log_rows(total)], axis=0)
     over_z.start()
+    relay(1, 2)
+    relay(2, 2)
     relay(3, 1)
-
-    with scope("diag"):
-        value32 = value.astype(F32)
-        in_block = lax.rem(lax.broadcasted_iota(jnp.int32, (T, 1), 0), 8)
-        decay = jnp.exp(logs)
-        weight = query
-        rec = jnp.sum(query * key, axis=1, keepdims=True) * value32
-        for d in range(1, 8):
-            weight = weight * (decay if d == 1 else pltpu.roll(decay, d - 1, 0))
-            score = jnp.sum(weight * pltpu.roll(key, d, 0), axis=1, keepdims=True)
-            rec = rec + jnp.where(in_block >= d, score, 0.0) * pltpu.roll(value32, d, 0)
-    relay(2, 2)
+    relay(1, 3)
+
     with scope("wait_z"):
         over_z.arrive()
     with scope("chain_z"):
@@ -429,7 +422,24 @@
             st3_out[k] = (jnp.exp(before[k]) * outer + inside[k]).astype(BF16)
     back.start()
     st3[y] = st3_out[y]
+    with scope("proj_qp"):
+        query = (mm(scaled, g1a[0].reshape(D, DK)) * inv_rms).astype(BF16)
+        query = query.astype(F32) * DK ** (-0.5)
+        pool = (mm(scaled, g1b[0].reshape(D, DK)) * inv_rms).astype(BF16)
+        rows_out[...] = pool[T - 16 :, :]
+    shift = remote(rows_out, rows_in, ps.at[0], pr.at[0], {Z: after_z, Y: after_y})
+    shift.start()
     relay(3, 2)
+    with scope("diag"):
+        value32 = value.astype(F32)
+        in_block = lax.rem(lax.broadcasted_iota(jnp.int32, (T, 1), 0), 8)
+        decay = jnp.exp(logs)
+        weight = query
+        rec = jnp.sum(query * key, axis=1, keepdims=True) * value32
+        for d in range(1, 8):
+            weight = weight * (decay if d == 1 else pltpu.roll(decay, d - 1, 0))
+            score = jnp.sum(weight * pltpu.roll(key, d, 0), axis=1, keepdims=True)
+            rec = rec + jnp.where(in_block >= d, score, 0.0) * pltpu.roll(value32, d, 0)
     with scope("levels"):
         scores = jnp.zeros((T, T), F32)
         for half in (8, 16, 32, 64, 128):
@@ -484,24 +494,10 @@
         )
 
     def sib_copy(side):
-        return pltpu.make_async_remote_copy(
-            src_ref=sib_out.at[side],
-            dst_ref=sib_in.at[side],
-            send_sem=bs.at[side],
-            recv_sem=br.at[side],
-            device_id={C: other},
-            device_id_type=MESH,
-        )
+        return remote(sib_out.at[side], sib_in.at[side], bs.at[0], br.at[side], {C: other})
 
     def red_copy(at, src, dst, step):
-        return pltpu.make_async_remote_copy(
-            src_ref=src,
-            dst_ref=dst,
-            send_sem=xs.at[at],
-            recv_sem=xr.at[at],
-            device_id={X: around(x + step, NX)},
-            device_id_type=MESH,
-        )
+        return remote(src, dst, xs.at[0], xr.at[at], {X: around(x + step, NX)})
 
     right, left, across = around(x + 1, NX), around(x - 1, NX), around(x + 2, NX)
     steps = (1, -1)
@@ -510,10 +506,10 @@
         [red_copy(2 * k + u, red_out.at[k, across, piece[u]], mid_in.at[k, piece[u]], steps[k]) for u in range(2)]
         for k in range(2)
     ]
-    near = [red_copy(4 + k, red_out.at[1 - k, (right, left)[k]], red_in.at[k], steps[k]) for k in range(2)]
+    near = [red_copy(4, red_out.at[1 - k, (right, left)[k]], red_in.at[k], steps[k]) for k in range(2)]
     merged = [
         [
-            red_copy(6 + 2 * k + u, red_out.at[k, (right, left)[k], piece[u]], red_in.at[2 + k, piece[u]], steps[k])
+            red_copy(4, red_out.at[k, (right, left)[k], piece[u]], red_in.at[2 + k, piece[u]], steps[k])
             for u in range(2)
         ]
         for k in range(2)
@@ -541,11 +537,7 @@
                 ).astype(BF16)
                 merged[k][u].start()
     with scope("red_wait"):
-        for k in range(2):
-            near[k].wait_recv()
-        for k in range(2):
-            for u in range(2):
-                merged[k][u].wait_recv()
+        red_copy(4, red_in, red_in, 1).wait_recv()
     with scope("final"):
         low = red_out[0, x].astype(F32) + red_in[2].astype(F32) + red_in[1].astype(F32)
         high = red_out[1, x].astype(F32) + red_in[0].astype(F32) + red_in[3].astype(F32)
@@ -555,16 +547,13 @@
         out[:, half_d:] = (high * scale * post[:, half_d:]).astype(BF16)
 
     with scope("drain"):
-        for stream in [one for pair in first + streams for one in pair] + [to_slices, over_z, back]:
-            stream.drain()
-        for distance in range(1, NX):
-            tok_out(distance).wait_send()
-            tok_copy(NX + distance, tok_from(distance) + c, {C: other}).wait_send()
-        tok_copy(0, tp, {C: other}).wait_send()
-        for k in range(2):
-            sib_copy(k).wait_send()
-        for copy in over[0] + over[1] + near + merged[0] + merged[1]:
-            copy.wait_send()
+        for one in [one for pair in streams for one in pair] + [to_slices, over_z, back]:
+            one.drain()
+        seven = xg.at[pl.ds(0, 2 * NX - 1)]
+        remote(seven, seven, ts.at[0], tr.at[0], {C: other}).wait_send()
+        remote(sib_out, sib_out, bs.at[0], br.at[0], {C: other}).wait_send()
+        six = red_out.at[:, pl.ds(0, NX - 1)]
+        remote(six, six, xs.at[0], xr.at[0], {X: right}).wait_send()
         shift.wait_send()
 
 
@@ -610,20 +599,22 @@
             pltpu.VMEM((2, OWN, D // 2), BF16),
             dma((9,)),
             dma((7,)),
-            dma((8, NR)),
-            dma((8, NR)),
-            dma((8, CUTS * NR)),
-            dma((8, CUTS * NR)),
-            dma((2 * NX,)),
-            dma((2 * NX,)),
-            dma((3, NR)),
-            dma((3, NR)),
+            dma((2, NR // 2)),
+            dma((2, 13)),
+            dma((8,)),
+            dma((6,)),
+            dma((8,)),
+            dma((6, 2 + CUTS * (NR - 3))),
+            dma((1,)),
+            dma((NX,)),
+            dma((3,)),
+            dma((3,)),
+            dma((1,)),
             dma((1,)),
             dma((1,)),
             dma((2,)),
-            dma((2,)),
-            dma((10,)),
-            dma((10,)),
+            dma((1,)),
+            dma((5,)),
         ],
         compiler_params=pltpu.CompilerParams(
             collective_id=0, has_side_effects=True, vmem_limit_bytes=32 * 1024 * 1024

time: 66.6 us -> 62.9 us (0.944)
  Pallas kernels: 65.8 us -> 62.1 us
    pallas_call x1, Pallas kernels: 65.8 us -> 62.1 us  [per_device(): run(*[pltpu.with_memory_space_constraint(a, pltpu.HBM) for a in operands])]
where the time goes in v4:
time: 62.9 us; the launch traced here: 62.8 us
  Pallas kernels  62.1 us (99%)
  local copies, waits for them, and re-layouts  0.66 us (1%)
    pallas_call x1, Pallas kernels, per_device(): run(*[pltpu.with_memory_space_constraint(a, pltpu.HBM) for a in operands])  62.1 us

profile of v4, /device:TPU:1, one launch (start us, length us, event | category | flops | bytes accessed | tf_op | source)
XLA Modules:
  0.0 62.8 jit_solution(3185497134780924563)
XLA Ops:
  0.0 62.1 %layer.1 = bf16[32,2048]{1,0:T(8,128)(2,1)S(1)} custom-call(bf16[256,256]{1,0:T(8,128)(2,1)} %tok.1, bf16[32,128]{1,0:T(8,128)(2,1)} %wq.1, bf16[32,128]{1,0:T(8,128)(2,1)} %wf.1, bf16[32,128]{1,0:T(8,128)(2,1)} %wi.1, bf16[32,128]{1,0:T(8,128)(2,1)} %wr.1, bf16[32,128]{1,0:T(8,128)(2,1)} %wp.1, bf16[32,128]{1,0:T(8,128)(2,1)} %wg.1, ...), custom_call_target="tpu_custom_call" | custom-call | tf_op jit(solution)/shard_map/layer/pallas_call | solution.py:641
  62.2 0.7 %copy.18 = bf16[32,2048]{1,0:T(8,128)(2,1)} copy(bf16[32,2048]{1,0:T(8,128)(2,1)S(1)} %layer.1) | data formatting | bytes 262144

commit v5 on v4

--- a/solution.py
+++ b/solution.py
@@ -66,21 +66,7 @@
         self.at, self.wide, self.long, self.w, self.l, self.sign = at, wide, long, w, l, sign
         self.send1, self.send2, self.recv1, self.recv2 = sems
 
-    def first_copy(self, distance, origin, recv):
-        block = self.at(pl.ds(origin, 1), pl.ds(self.l, 1))
-        return remote(block, block, self.send1, recv, {self.wide: around(self.w + distance, NR)})
-
-    def first_start(self):
-        for distance in ORDER:
-            self.first_copy(distance, self.w, self.recv1).start()
-
-    def first_arrive(self):
-        view = self.at(pl.ds(0, NR - 1), pl.ds(self.l, 1))
-        remote(view, view, self.send1, self.recv1, {self.wide: around(self.w + 1, NR)}).wait_recv()
-
     def drain(self):
-        view = self.at(pl.ds(0, NR - 1), pl.ds(self.l, 1))
-        remote(view, view, self.send1, self.send1, {self.wide: around(self.w + 1, NR)}).wait_send()
         view = self.at(pl.ds(0, NR), pl.ds(0, NR - 1))
         remote(view, view, self.send2, self.send2, {self.long: around(self.l + 1, NR)}).wait_send()
 
@@ -116,16 +102,49 @@
             remote(block, block, self.send2, self.sem(step, back, cut), where).wait_recv()
 
 
+class Leaps:
+    def __init__(self, part, axis, me, sign, send, recv):
+        self.part, self.axis, self.me, self.sign, self.send, self.recv = part, axis, me, sign, send, recv
+
+    def copy(self, move, origin, sem, count=1):
+        block = self.part(origin, count)
+        where = {self.axis: around(self.me + self.sign * move, NR)}
+        return remote(block, block, self.send, self.recv.at[sem], where)
+
+    def start(self):
+        for move, sem in ((2, 0), (-2, 1), (1, 2), (-1, 2)):
+            self.copy(move, self.me, sem).start()
+
+    def go_on(self):
+        origin = around(self.me - 2 * self.sign, NR)
+        self.copy(2, origin, 0).wait_recv()
+        self.copy(2, origin, 2).start()
+        self.copy(1, origin, 2).start()
+        origin = around(self.me + 2 * self.sign, NR)
+        self.copy(-2, origin, 1).wait_recv()
+        self.copy(-1, origin, 2).start()
+
+    def arrive(self):
+        self.copy(1, 0, 2, 5).wait_recv()
+
+    def drain(self):
+        self.copy(1, 0, 2, 7).wait_send()
+
+
 class FastStream(Stream):
+    def drain(self):
+        view = self.at(pl.ds(0, NR - 1), pl.ds(self.l, 1))
+        remote(view, view, self.send1, self.send1, {self.wide: around(self.w + 1, NR)}).wait_send()
+        Stream.drain(self)
+
     def first_start(self):
         pair, twin = self.w // 2, self.w + 1 - 2 * lax.rem(self.w, 2)
+        block = self.at(pl.ds(self.w, 1), pl.ds(self.l, 1))
+        remote(block, block, self.send1, self.recv1.at[0], {self.wide: twin}).start()
         for ahead in (2, 1, 3):
             for k in range(2):
                 place = 2 * lax.rem(pair + ahead, NR // 2) + k
-                block = self.at(pl.ds(self.w, 1), pl.ds(self.l, 1))
                 remote(block, block, self.send1, self.recv1.at[NR // 2 - ahead], {self.wide: place}).start()
-        block = self.at(pl.ds(self.w, 1), pl.ds(self.l, 1))
-        remote(block, block, self.send1, self.recv1.at[0], {self.wide: twin}).start()
 
     def pair_at(self, ahead):
         return 2 * lax.rem(self.w // 2 + ahead, NR // 2)
@@ -205,7 +224,7 @@
     out,
     g0a, g0b, g1a, g1b, xg, sc,
     ngain, rate, extra, sgain, pmix, pgain, post,
-    st_out, st1, st2, st3_out, st3, rows_out, rows_in, yb, sib_out, sib_in, red_out, red_in, mid_in,
+    st_out, st1, st2, st3_out, st3, rows_out, rows_in, yb, early, sib_out, sib_in, red_out, red_in, mid_in,
     lsem, vsem, f1r, f2r, p1s, p1r, p2s, p2r, ts, tr, ss, sr, ps, pr, bs, br, xs, xr,
 ):
     scope = jax.named_scope
@@ -264,7 +283,7 @@
         pl.semaphore_wait(barrier, 2 * (NR - 1) + NX - 1 + 2)
 
     def stream(kind, buffer, flip, at, recv1, recv2):
-        sems = (p1s.at[at], p2s.at[at], recv1, recv2)
+        sems = (p1s.at[flip], p2s.at[at], recv1, recv2)
         if flip:
             return kind(lambda w, l: buffer.at[w, l], Z, Y, z, y, sign, sems)
         return kind(lambda w, l: buffer.at[l, w], Y, Z, y, z, sign, sems)
@@ -273,21 +292,23 @@
         stream(FastStream, buffer, flip, flip, f1r.at[flip], f2r.at[flip])
         for flip, buffer in enumerate((g0a, g0b))
     ]
-    streams = [
+    streams = [fast] + [
         [
-            stream(Stream, buffer.at[k], flip, 2 * k + 2 + flip, p1r.at[2 * k + flip], p2r.at[2 * k + flip])
+            stream(Stream, buffer.at[k], flip, 2 * k + 2 + flip, None, p2r.at[2 * k + flip])
             for flip, buffer in enumerate((g1a, g1b))
         ]
         for k in range(3)
     ]
-    streams = [fast] + streams
+    rest = [
+        Leaps(lambda o, n: g1a.at[:, z, pl.ds(o, n)], Y, y, sign, p1s.at[2], p1r.at[0]),
+        Leaps(lambda o, n: g1b.at[:, pl.ds(o, n), y], Z, z, sign, p1s.at[3], p1r.at[1]),
+    ]
 
     def start(k):
         with scope("first%d" % k):
-            for one in streams[k]:
-                one.first_arrive()
-                for cut in range(CUTS):
-                    for back in (False, True):
+            for cut in range(CUTS):
+                for back in (False, True):
+                    for one in streams[k]:
                         one.start(0, back, cut)
 
     def relay(k, step):
@@ -296,10 +317,6 @@
                 for back in (False, True):
                     for one in streams[k]:
                         one.relay(step, back, cut)
-
-    def first_start(k):
-        for one in streams[k]:
-            one.first_start()
 
     def tok_copy(at, slot, where):
         return remote(xg.at[slot], xg.at[slot], ts.at[0], tr.at[at], where)
@@ -318,8 +335,8 @@
         tok_copy(0, tp, {C: other}).start()
         for k in range(3, 9):
             local[k].wait()
-        first_start(1)
-        first_start(2)
+        for one in rest:
+            one.start()
         for copy in vectors:
             copy.wait()
 
@@ -328,17 +345,23 @@
             for one in fast:
                 one.first_arrive(ahead)
                 one.send_own(ahead)
+    with scope("leap"):
+        for one in rest:
+            one.go_on()
+    for ahead in (0, 1, 3, 2):
+        with scope("on%d" % ahead):
+            for one in fast:
+                one.send_on(ahead)
     with scope("tokens"):
         for distance in (1, 3, 2):
             tok_copy(distance, tok_from(distance) + c, {X: around(x + distance, NX)}).wait_recv()
             tok_copy(0, tok_from(distance) + c, {C: other}).start()
-    for ahead in (0, 1, 3, 2):
-        with scope("on%d" % ahead):
-            for one in fast:
-                one.send_on(ahead)
+    with scope("rest"):
+        for one in rest:
+            one.arrive()
     start(1)
-    first_start(3)
     start(2)
+    start(3)
     with scope("tokens2"):
         four = xg.at[pl.ds(0, NX)]
         remote(four, four, ts.at[0], tr.at[0], {C: other}).wait_recv()
@@ -387,10 +410,9 @@
     to_slices.start()
     st1[y] = st_out[y]
     relay(2, 0)
-    start(3)
+    relay(3, 0)
     relay(1, 1)
     relay(2, 1)
-    relay(3, 0)
     with scope("wait_y"):
         to_slices.arrive()
     with scope("chain_y"):
@@ -404,11 +426,9 @@
             total = total + new_total
         st2[z] = jnp.concatenate([state.astype(BF16), log_rows(total)], axis=0)
     over_z.start()
+    relay(3, 1)
     relay(1, 2)
     relay(2, 2)
-    relay(3, 1)
-    relay(1, 3)
-
     with scope("wait_z"):
         over_z.arrive()
     with scope("chain_z"):
@@ -422,6 +442,8 @@
             st3_out[k] = (jnp.exp(before[k]) * outer + inside[k]).astype(BF16)
     back.start()
     st3[y] = st3_out[y]
+    relay(3, 2)
+    relay(1, 3)
     with scope("proj_qp"):
         query = (mm(scaled, g1a[0].reshape(D, DK)) * inv_rms).astype(BF16)
         query = query.astype(F32) * DK ** (-0.5)
@@ -429,7 +451,7 @@
         rows_out[...] = pool[T - 16 :, :]
     shift = remote(rows_out, rows_in, ps.at[0], pr.at[0], {Z: after_z, Y: after_y})
     shift.start()
-    relay(3, 2)
+    relay(2, 3)
     with scope("diag"):
         value32 = value.astype(F32)
         in_block = lax.rem(lax.broadcasted_iota(jnp.int32, (T, 1), 0), 8)
@@ -469,29 +491,30 @@
         mixed = (sums[16:] / count - pool32).astype(BF16)
         mapped = mm(mixed, pmix[...]) * pgain[...]
         faded = query * jnp.exp(cum)
-    relay(2, 3)
     with scope("proj_rg"):
         rgate = (mm(scaled, g1a[1].reshape(D, DK)) * inv_rms).astype(BF16).astype(F32)
         pgate = (mm(scaled, g1b[1].reshape(D, DK)) * inv_rms).astype(BF16).astype(F32)
         y_pool = (mapped * silu(pgate)).astype(BF16)
         gate = sgain[...] * silu(rgate)
     relay(3, 3)
+    half_d = D // 2
+
+    def project(left, weight, side):
+        at = slice(side * (NR // 2), (side + 1) * (NR // 2))
+        return mm(left, weight[2, at].reshape(half_d, DK), 1, 1)
+
+    with scope("pooled"):
+        yb[...] = y_pool.reshape(NX, 2, OWN, DK)
+        for k, parity in enumerate((other, c)):
+            for side in range(2):
+                early[k, side] = project(yb[:, parity].reshape(NX * OWN, DK), g1b, side)
     with scope("wait_back"):
         back.arrive()
     with scope("rec"):
         rec = rec + mm2(faded, st3[...].reshape(DK, DK), 1, 1)
         normed = rec * lax.rsqrt(jnp.mean(rec * rec, axis=1, keepdims=True) + EPS)
         y_rec = (normed * gate).astype(BF16)
-        yb[...] = jnp.concatenate([y_rec, y_pool], axis=1).reshape(NX, 2, OWN, 2 * DK)
-
-    half_d = D // 2
-
-    def project(parity, side):
-        left = yb[:, parity].reshape(NX * OWN, 2 * DK)
-        at = slice(side * (NR // 2), (side + 1) * (NR // 2))
-        return mm(left[:, :DK], g1a[2, at].reshape(half_d, DK), 1, 1) + mm(
-            left[:, DK:], g1b[2, at].reshape(half_d, DK), 1, 1
-        )
+        yb[...] = y_rec.reshape(NX, 2, OWN, DK)
 
     def sib_copy(side):
         return remote(sib_out.at[side], sib_in.at[side], bs.at[0], br.at[side], {C: other})
@@ -516,11 +539,13 @@
     ]
     with scope("proj_sib"):
         for side in range(2):
-            sib_out[side] = project(other, side).astype(BF16).reshape(NX, OWN, half_d)
+            part = early[0, side] + project(yb[:, other].reshape(NX * OWN, DK), g1a, side)
+            sib_out[side] = part.astype(BF16).reshape(NX, OWN, half_d)
             sib_copy(side).start()
     with scope("proj_mine"):
         for side in range(2):
-            part = project(c, side).reshape(NX, OWN, half_d)
+            part = early[1, side] + project(yb[:, c].reshape(NX * OWN, DK), g1a, side)
+            part = part.reshape(NX, OWN, half_d)
             sib_copy(side).wait_recv()
             red_out[side] = (part + sib_in[side].astype(F32)).astype(BF16)
             for u in range(2):
@@ -547,7 +572,7 @@
         out[:, half_d:] = (high * scale * post[:, half_d:]).astype(BF16)
 
     with scope("drain"):
-        for one in [one for pair in streams for one in pair] + [to_slices, over_z, back]:
+        for one in [one for pair in streams for one in pair] + rest + [to_slices, over_z, back]:
             one.drain()
         seven = xg.at[pl.ds(0, 2 * NX - 1)]
         remote(seven, seven, ts.at[0], tr.at[0], {C: other}).wait_send()
@@ -591,7 +616,8 @@
             pltpu.VMEM((NR, 16, DK), BF16),
             pltpu.VMEM((16, DK), BF16),
             pltpu.VMEM((16, DK), BF16),
-            pltpu.VMEM((NX, 2, OWN, 2 * DK), BF16),
+            pltpu.VMEM((NX, 2, OWN, DK), BF16),
+            pltpu.VMEM((2, 2, NX * OWN, D // 2), F32),
             pltpu.VMEM((2, NX, OWN, D // 2), BF16),
             pltpu.VMEM((2, NX, OWN, D // 2), BF16),
             pltpu.VMEM((2, NX, OWN, D // 2), BF16),
@@ -601,8 +627,8 @@
             dma((7,)),
             dma((2, NR // 2)),
             dma((2, 13)),
-            dma((8,)),
-            dma((6,)),
+            dma((4,)),
+            dma((2, 3)),
             dma((8,)),
             dma((6, 2 + CUTS * (NR - 3))),
             dma((1,)),

time: 62.9 us -> 61.1 us (0.971)
  Pallas kernels: 62.1 us -> 60.3 us
    pallas_call x1, Pallas kernels: 62.1 us -> 60.3 us  [per_device(): run(*[pltpu.with_memory_space_constraint(a, pltpu.HBM) for a in operands])]
where the time goes in v5:
time: 61.1 us; the launch traced here: 61 us
  Pallas kernels  60.3 us (99%)
  local copies, waits for them, and re-layouts  0.66 us (1%)
    pallas_call x1, Pallas kernels, per_device(): run(*[pltpu.with_memory_space_constraint(a, pltpu.HBM) for a in operands])  60.3 us

profile of v5, /device:TPU:1, one launch (start us, length us, event | category | flops | bytes accessed | tf_op | source)
XLA Modules:
  0.0 61.0 jit_solution(17494047377629148256)
XLA Ops:
  0.0 60.3 %layer.1 = bf16[32,2048]{1,0:T(8,128)(2,1)S(1)} custom-call(bf16[256,256]{1,0:T(8,128)(2,1)} %tok.1, bf16[32,128]{1,0:T(8,128)(2,1)} %wq.1, bf16[32,128]{1,0:T(8,128)(2,1)} %wf.1, bf16[32,128]{1,0:T(8,128)(2,1)} %wi.1, bf16[32,128]{1,0:T(8,128)(2,1)} %wr.1, bf16[32,128]{1,0:T(8,128)(2,1)} %wp.1, bf16[32,128]{1,0:T(8,128)(2,1)} %wg.1, ...), custom_call_target="tpu_custom_call" | custom-call | tf_op jit(solution)/shard_map/layer/pallas_call | solution.py:667
  60.3 0.7 %copy.18 = bf16[32,2048]{1,0:T(8,128)(2,1)} copy(bf16[32,2048]{1,0:T(8,128)(2,1)S(1)} %layer.1) | data formatting | bytes 262144

commit v6 on v5

--- a/solution.py
+++ b/solution.py
@@ -36,12 +36,6 @@
     return hi, (a - hi.astype(F32)).astype(BF16)
 
 
-def mm3(a, b, ca=1, cb=0):
-    ah, al = halves(a)
-    bh, bl = halves(b)
-    return mm(ah, bh, ca, cb) + (mm(ah, bl, ca, cb) + mm(al, bh, ca, cb))
-
-
 def mm2(a, b, ca=1, cb=0):
     ah, al = halves(a)
     return mm(ah, b, ca, cb) + mm(al, b, ca, cb)
@@ -92,14 +86,12 @@
         if step < self.steps(back):
             self.copy(step, back, cut, self.origin(step, back)).start()
 
-    def relay(self, step, back, cut):
-        if step < self.steps(back) - 1:
-            self.copy(step, back, cut, self.origin(step + 1, back)).wait_recv()
-            self.start(step + 1, back, cut)
-        elif step == self.steps(back) - 1 and cut == CUTS - 1:
-            block = self.at(pl.ds(0, NR), pl.ds(self.origin(step + 1, back), 1))
+    def arrive(self, step, back, cut):
+        last = step == self.steps(back) - 1
+        if step < self.steps(back) and (not last or cut == CUTS - 1):
+            view = self.at(pl.ds(0, NR), pl.ds(0, 2)) if last else self.at(pl.ds(0, 2 * SPAN), pl.ds(0, 1))
             where = {self.long: around(self.l + self.sign, NR)}
-            remote(block, block, self.send2, self.sem(step, back, cut), where).wait_recv()
+            remote(view, view, self.send2, self.sem(step, back, cut), where).wait_recv()
 
 
 class Leaps:
@@ -149,37 +141,40 @@
     def pair_at(self, ahead):
         return 2 * lax.rem(self.w // 2 + ahead, NR // 2)
 
+    def wait(self, view, sem):
+        where = {self.long: around(self.l + self.sign, NR)}
+        remote(view, view, self.send2, sem, where).wait_recv()
+
     def first_arrive(self, ahead):
-        twin = self.w + 1 - 2 * lax.rem(self.w, 2)
-        if ahead == 0:
-            view = self.at(pl.ds(twin, 1), pl.ds(self.l, 1))
-        else:
-            view = self.at(pl.ds(self.pair_at(ahead), 2), pl.ds(self.l, 1))
-        remote(view, view, self.send1, self.recv1.at[ahead], {self.wide: twin}).wait_recv()
+        self.wait(self.at(pl.ds(0, 4 if ahead else 2), pl.ds(0, 1)), self.recv1.at[ahead])
+
+    def arrive(self, ahead, back):
+        self.wait(self.at(pl.ds(0, 4), pl.ds(0, 1)), self.recv2.at[(9 if back else 5) + ahead])
+
+    def finish(self):
+        for sem in (0, 3, 1, 4, 2):
+            self.wait(self.at(pl.ds(0, NR), pl.ds(0, 2)), self.recv2.at[sem])
 
     def hop(self, ahead, origin, move, sem):
         block = self.at(pl.ds(self.pair_at(ahead), 2), pl.ds(origin, 1))
         where = {self.long: around(self.l + self.sign * move, NR)}
         return remote(block, block, self.send2, self.recv2.at[sem], where)
 
-    def send_own(self, ahead):
-        for move, sem in ((2, 5 + ahead), (-2, 9 + ahead), (1, 0), (-1, 3)):
-            self.hop(ahead, self.l, move, sem).start()
-
-    def send_on(self, ahead):
-        origin = around(self.l - 2 * self.sign, NR)
-        self.hop(ahead, origin, 2, 5 + ahead).wait_recv()
-        self.hop(ahead, origin, 2, 2).start()
-        self.hop(ahead, origin, 1, 1).start()
-        origin = around(self.l + 2 * self.sign, NR)
-        self.hop(ahead, origin, -2, 9 + ahead).wait_recv()
-        self.hop(ahead, origin, -1, 4).start()
-
-    def finish(self):
-        for move, sem in ((1, 0), (-1, 3), (3, 1), (-3, 4), (4, 2)):
-            block = self.at(pl.ds(0, NR), pl.ds(around(self.l - self.sign * move, NR), 1))
-            where = {self.long: around(self.l + self.sign, NR)}
-            remote(block, block, self.send2, self.recv2.at[sem], where).wait_recv()
+    def send_two(self, ahead):
+        self.hop(ahead, self.l, 2, 5 + ahead).start()
+        self.hop(ahead, self.l, -2, 9 + ahead).start()
+
+    def send_one(self, ahead):
+        self.hop(ahead, self.l, 1, 0).start()
+        self.hop(ahead, self.l, -1, 3).start()
+
+    def send_on(self, ahead, back):
+        if back:
+            self.hop(ahead, around(self.l + 2 * self.sign, NR), -1, 4).start()
+        else:
+            origin = around(self.l - 2 * self.sign, NR)
+            self.hop(ahead, origin, 2, 2).start()
+            self.hop(ahead, origin, 1, 1).start()
 
 
 class Direct:
@@ -203,11 +198,15 @@
         self.whole().wait_send()
 
 
+def thirds(a):
+    hi = a.astype(BF16)
+    rest = a - hi.astype(F32)
+    mid = rest.astype(BF16)
+    return hi, mid, (rest - mid.astype(F32)).astype(BF16)
+
+
 def log_rows(total):
-    hi = total.astype(BF16)
-    rest = total - hi.astype(F32)
-    mid = rest.astype(BF16)
-    low = (rest - mid.astype(F32)).astype(BF16)
+    hi, mid, low = thirds(total)
     place = lax.broadcasted_iota(jnp.int32, (16, DK), 0)
     parts = jnp.where(place == 1, mid.astype(F32), jnp.where(place == 2, low.astype(F32), 0.0))
     return jnp.where(place == 0, hi.astype(F32), parts).astype(BF16)
@@ -249,18 +248,16 @@
 
     local = [
         pltpu.make_async_copy(src, dst, lsem.at[k])
-        for k, (src, dst) in enumerate(
-            (
-                (wf, g0a.at[z, y]),
-                (wi, g0b.at[z, y]),
-                (tok, xg.at[tp]),
-                (wq, g1a.at[0, z, y]),
-                (wr, g1a.at[1, z, y]),
-                (orec, g1a.at[2, z, y]),
-                (wp, g1b.at[0, z, y]),
-                (wg, g1b.at[1, z, y]),
-                (opool, g1b.at[2, z, y]),
-            )
+        for k, src, dst in (
+            (0, wf, g0a.at[z, y]),
+            (1, wi, g0b.at[z, y]),
+            (2, tok, xg.at[tp]),
+            (3, wq, g1a.at[0, z, y]),
+            (3, wr, g1a.at[1, z, y]),
+            (3, orec, g1a.at[2, z, y]),
+            (4, wp, g1b.at[0, z, y]),
+            (4, wg, g1b.at[1, z, y]),
+            (4, opool, g1b.at[2, z, y]),
         )
     ]
     vectors = [
@@ -289,12 +286,12 @@
         return kind(lambda w, l: buffer.at[l, w], Y, Z, y, z, sign, sems)
 
     fast = [
-        stream(FastStream, buffer, flip, flip, f1r.at[flip], f2r.at[flip])
+        stream(FastStream, buffer, flip, flip, f1r, f2r)
         for flip, buffer in enumerate((g0a, g0b))
     ]
     streams = [fast] + [
         [
-            stream(Stream, buffer.at[k], flip, 2 * k + 2 + flip, None, p2r.at[2 * k + flip])
+            stream(Stream, buffer.at[k], flip, 2 * k + 2 + flip, None, p2r.at[k])
             for flip, buffer in enumerate((g1a, g1b))
         ]
         for k in range(3)
@@ -315,8 +312,9 @@
         with scope("relay%d%d" % (k, step)):
             for cut in range(CUTS):
                 for back in (False, True):
+                    streams[k][0].arrive(step, back, cut)
                     for one in streams[k]:
-                        one.relay(step, back, cut)
+                        one.start(step + 1, back, cut)
 
     def tok_copy(at, slot, where):
         return remote(xg.at[slot], xg.at[slot], ts.at[0], tr.at[at], where)
@@ -333,8 +331,8 @@
         for distance in (2, 1, 3):
             tok_copy(distance, tp, {X: around(x + distance, NX)}).start()
         tok_copy(0, tp, {C: other}).start()
-        for k in range(3, 9):
-            local[k].wait()
+        pltpu.make_async_copy(g1a.at[:, z, y], g1a.at[:, z, y], lsem.at[3]).wait()
+        pltpu.make_async_copy(g1b.at[:, z, y], g1b.at[:, z, y], lsem.at[4]).wait()
         for one in rest:
             one.start()
         for copy in vectors:
@@ -342,16 +340,21 @@
 
     for ahead in (0, 1, 3, 2):
         with scope("own%d" % ahead):
+            fast[0].first_arrive(ahead)
             for one in fast:
-                one.first_arrive(ahead)
-                one.send_own(ahead)
+                one.send_two(ahead)
+    for ahead in (0, 1, 3, 2):
+        for one in fast:
+            one.send_one(ahead)
     with scope("leap"):
         for one in rest:
             one.go_on()
     for ahead in (0, 1, 3, 2):
         with scope("on%d" % ahead):
-            for one in fast:
-                one.send_on(ahead)
+            for back in (False, True):
+                fast[0].arrive(ahead, back)
+                for one in fast:
+                    one.send_on(ahead, back)
     with scope("tokens"):
         for distance in (1, 3, 2):
             tok_copy(distance, tok_from(distance) + c, {X: around(x + distance, NX)}).wait_recv()
@@ -373,20 +376,6 @@
             at = slice(k * (D // (2 * NX)), (k + 1) * (D // (2 * NX)))
             sc[:, at] = (block * ngain[:, at]).astype(BF16)
         inv_rms = lax.rsqrt(squares * (1.0 / D) + EPS)
-    with scope("finish"):
-        for one in fast:
-            one.finish()
-
-    with scope("proj_fv"):
-        scaled = sc[...]
-        forget = (mm(scaled, g0a[...].reshape(D, DK)) * inv_rms).astype(BF16).astype(F32)
-        value = (mm(scaled, g0b[...].reshape(D, DK)) * inv_rms).astype(BF16)
-    relay(1, 0)
-    with scope("gates"):
-        r = rate[...]
-        series = r * (1.0 - r / 2 * (1.0 - r / 3 * (1.0 - r / 4 * (1.0 - r / 5 * (1.0 - r / 6)))))
-        reach = jnp.where(r < 0.1, series, 1.0 - jnp.exp(-r))
-        key = reach * (1.0 / (1.0 + jnp.exp(forget)))
         more = lax.dot_general(
             extra[...],
             jnp.ones((1, DK), F32),
@@ -394,13 +383,27 @@
             precision=lax.Precision.HIGHEST,
             preferred_element_type=F32,
         )
-        logs = jnp.log1p(-key) + more
         row = lax.broadcasted_iota(jnp.int32, (T, T), 0)
         col = lax.broadcasted_iota(jnp.int32, (T, T), 1)
-        lower = jnp.where(row >= col, 1.0, 0.0)
-        cum = jnp.dot(lower, logs, precision=lax.Precision.HIGHEST, preferred_element_type=F32)
+        lower = jnp.where(row >= col, 1.0, 0.0).astype(BF16)
+    with scope("finish"):
+        fast[0].finish()
+
+    with scope("proj_fv"):
+        scaled = sc[...]
+        forget = (mm(scaled, g0a[...].reshape(D, DK)) * inv_rms).astype(BF16).astype(F32)
+        value = (mm(scaled, g0b[...].reshape(D, DK)) * inv_rms).astype(BF16)
+    with scope("gates"):
+        r = rate[...]
+        series = r * (1.0 - r / 2 * (1.0 - r / 3 * (1.0 - r / 4 * (1.0 - r / 5 * (1.0 - r / 6)))))
+        reach = jnp.where(r < 0.1, series, 1.0 - jnp.exp(-r))
+        key = reach * (1.0 / (1.0 + jnp.exp(forget)))
+        logs = jnp.log1p(-key) + more
+        cum = mm(lower, jnp.concatenate(thirds(logs), axis=1))
+        cum = cum[:, :DK] + (cum[:, DK : 2 * DK] + cum[:, 2 * DK :])
         last = cum[T - 1 : T, :]
-        memory = mm2(key * jnp.exp(last - cum), value, 0, 0).T
+        hi, low = halves(key * jnp.exp(last - cum))
+        memory = mm(value, hi, 0, 0) + mm(value, low, 0, 0)
         st_out[:, 0:16] = memory.astype(BF16).reshape(NR, 16, DK)
         st_out[:, 16:32] = jnp.broadcast_to(log_rows(last)[None], (NR, 16, DK))
 
@@ -409,10 +412,10 @@
     back = Direct(st3, Y, y, ss.at[2], sr.at[2], st3_out)
     to_slices.start()
     st1[y] = st_out[y]
+    relay(1, 0)
     relay(2, 0)
     relay(3, 0)
     relay(1, 1)
-    relay(2, 1)
     with scope("wait_y"):
         to_slices.arrive()
     with scope("chain_y"):
@@ -426,9 +429,9 @@
             total = total + new_total
         st2[z] = jnp.concatenate([state.astype(BF16), log_rows(total)], axis=0)
     over_z.start()
+    relay(2, 1)
     relay(3, 1)
     relay(1, 2)
-    relay(2, 2)
     with scope("wait_z"):
         over_z.arrive()
     with scope("chain_z"):
@@ -442,16 +445,17 @@
             st3_out[k] = (jnp.exp(before[k]) * outer + inside[k]).astype(BF16)
     back.start()
     st3[y] = st3_out[y]
-    relay(3, 2)
+    relay(2, 2)
     relay(1, 3)
-    with scope("proj_qp"):
-        query = (mm(scaled, g1a[0].reshape(D, DK)) * inv_rms).astype(BF16)
-        query = query.astype(F32) * DK ** (-0.5)
+    with scope("proj_p"):
         pool = (mm(scaled, g1b[0].reshape(D, DK)) * inv_rms).astype(BF16)
         rows_out[...] = pool[T - 16 :, :]
     shift = remote(rows_out, rows_in, ps.at[0], pr.at[0], {Z: after_z, Y: after_y})
     shift.start()
-    relay(2, 3)
+    relay(3, 2)
+    with scope("proj_q"):
+        query = (mm(scaled, g1a[0].reshape(D, DK)) * inv_rms).astype(BF16)
+        query = query.astype(F32) * DK ** (-0.5)
     with scope("diag"):
         value32 = value.astype(F32)
         in_block = lax.rem(lax.broadcasted_iota(jnp.int32, (T, 1), 0), 8)
@@ -468,10 +472,15 @@
             apart = cum.reshape(T // (2 * half), 2 * half, DK)
             apart = jnp.abs(apart - apart[:, half - 1 : half, :]).reshape(T, DK)
             fade = jnp.exp(-apart)
-            level = mm3(query * fade, key * fade, 1, 1)
+            level = mm((query * fade).astype(BF16), (key * fade).astype(BF16), 1, 1)
             mask = (row // (2 * half) == col // (2 * half)) & (row // half > col // half)
             scores = jnp.where(mask, level, scores)
         rec = rec + mm2(scores, value)
+    relay(2, 3)
+    with scope("proj_rg"):
+        rgate = (mm(scaled, g1a[1].reshape(D, DK)) * inv_rms).astype(BF16).astype(F32)
+        pgate = (mm(scaled, g1b[1].reshape(D, DK)) * inv_rms).astype(BF16).astype(F32)
+        gate = sgain[...] * silu(rgate)
     with scope("pool"):
         shift.wait_recv()
         at_start = (z == 0) & (y == 0)
@@ -491,11 +500,7 @@
         mixed = (sums[16:] / count - pool32).astype(BF16)
         mapped = mm(mixed, pmix[...]) * pgain[...]
         faded = query * jnp.exp(cum)
-    with scope("proj_rg"):
-        rgate = (mm(scaled, g1a[1].reshape(D, DK)) * inv_rms).astype(BF16).astype(F32)
-        pgate = (mm(scaled, g1b[1].reshape(D, DK)) * inv_rms).astype(BF16).astype(F32)
         y_pool = (mapped * silu(pgate)).astype(BF16)
-        gate = sgain[...] * silu(rgate)
     relay(3, 3)
     half_d = D // 2
 
@@ -623,14 +628,14 @@
             pltpu.VMEM((2, NX, OWN, D // 2), BF16),
             pltpu.VMEM((4, OWN, D // 2), BF16),
             pltpu.VMEM((2, OWN, D // 2), BF16),
-            dma((9,)),
+            dma((5,)),
             dma((7,)),
-            dma((2, NR // 2)),
-            dma((2, 13)),
+            dma((NR // 2,)),
+            dma((13,)),
             dma((4,)),
             dma((2, 3)),
             dma((8,)),
-            dma((6, 2 + CUTS * (NR - 3))),
+            dma((3, 2 + CUTS * (NR - 3))),
             dma((1,)),
             dma((NX,)),
             dma((3,)),

time: 61.1 us -> 59.2 us (0.969)
  Pallas kernels: 60.3 us -> 58.5 us
    pallas_call x1, Pallas kernels: 60.3 us -> 58.5 us  [per_device(): run(*[pltpu.with_memory_space_constraint(a, pltpu.HBM) for a in operands])]
where the time goes in v6:
time: 59.2 us; the launch traced here: 59.1 us
  Pallas kernels  58.5 us (99%)
  local copies, waits for them, and re-layouts  0.66 us (1%)
    pallas_call x1, Pallas kernels, per_device(): run(*[pltpu.with_memory_space_constraint(a, pltpu.HBM) for a in operands])  58.5 us

profile of v6, /device:TPU:1, one launch (start us, length us, event | category | flops | bytes accessed | tf_op | source)
XLA Modules:
  0.0 59.1 jit_solution(7780987784377696493)
XLA Ops:
  0.0 58.5 %layer.1 = bf16[32,2048]{1,0:T(8,128)(2,1)S(1)} custom-call(bf16[256,256]{1,0:T(8,128)(2,1)} %tok.1, bf16[32,128]{1,0:T(8,128)(2,1)} %wq.1, bf16[32,128]{1,0:T(8,128)(2,1)} %wf.1, bf16[32,128]{1,0:T(8,128)(2,1)} %wi.1, bf16[32,128]{1,0:T(8,128)(2,1)} %wr.1, bf16[32,128]{1,0:T(8,128)(2,1)} %wp.1, bf16[32,128]{1,0:T(8,128)(2,1)} %wg.1, ...), custom_call_target="tpu_custom_call" | custom-call | tf_op jit(solution)/shard_map/layer/pallas_call | solution.py:672
  58.5 0.7 %copy.18 = bf16[32,2048]{1,0:T(8,128)(2,1)} copy(bf16[32,2048]{1,0:T(8,128)(2,1)S(1)} %layer.1) | data formatting | bytes 262144

commit v7 on v6

--- a/solution.py
+++ b/solution.py
@@ -207,7 +207,7 @@
 
 def log_rows(total):
     hi, mid, low = thirds(total)
-    place = lax.broadcasted_iota(jnp.int32, (16, DK), 0)
+    place = lax.broadcasted_iota(jnp.int32, (8, DK), 0)
     parts = jnp.where(place == 1, mid.astype(F32), jnp.where(place == 2, low.astype(F32), 0.0))
     return jnp.where(place == 0, hi.astype(F32), parts).astype(BF16)
 
@@ -223,8 +223,8 @@
     out,
     g0a, g0b, g1a, g1b, xg, sc,
     ngain, rate, extra, sgain, pmix, pgain, post,
-    st_out, st1, st2, st3_out, st3, rows_out, rows_in, yb, early, sib_out, sib_in, red_out, red_in, mid_in,
-    lsem, vsem, f1r, f2r, p1s, p1r, p2s, p2r, ts, tr, ss, sr, ps, pr, bs, br, xs, xr,
+    st_out, st1, st2, st3_out, st3, rows_out, rows_in, yb, yo, yi, early, o2a, o2b, red_out, red_in, mid_in,
+    lsem, vsem, f1r, f2r, p1s, p1r, p2s, p2r, ts, tr, ss, sr, ps, pr, bs, br, cs, cr, xs, xr,
 ):
     scope = jax.named_scope
     z, y, x, c = lax.axis_index(Z), lax.axis_index(Y), lax.axis_index(X), lax.axis_index(C)
@@ -316,6 +316,15 @@
                     for one in streams[k]:
                         one.start(step + 1, back, cut)
 
+    def pass_on(step):
+        for k, (src, dst) in enumerate(((g1a, o2a), (g1b, o2b))):
+            me = (z, y)[k]
+            for move in sorted({step, -step}) if step < NR // 2 else [step * sign]:
+                o = around(me + move, NR)
+                place = (2, o) if k == 0 else (2, slice(None), o)
+                to = (o,) if k == 0 else (slice(None), o)
+                remote(src.at[place], dst.at[to], cs.at[k], cr.at[k], {C: other}).start()
+
     def tok_copy(at, slot, where):
         return remote(xg.at[slot], xg.at[slot], ts.at[0], tr.at[at], where)
 
@@ -365,6 +374,7 @@
     start(1)
     start(2)
     start(3)
+    pass_on(0)
     with scope("tokens2"):
         four = xg.at[pl.ds(0, NX)]
         remote(four, four, ts.at[0], tr.at[0], {C: other}).wait_recv()
@@ -405,7 +415,7 @@
         hi, low = halves(key * jnp.exp(last - cum))
         memory = mm(value, hi, 0, 0) + mm(value, low, 0, 0)
         st_out[:, 0:16] = memory.astype(BF16).reshape(NR, 16, DK)
-        st_out[:, 16:32] = jnp.broadcast_to(log_rows(last)[None], (NR, 16, DK))
+        st_out[:, 16:24] = jnp.broadcast_to(log_rows(last)[None], (NR, 8, DK))
 
     to_slices = Direct(st1, Y, y, ss.at[0], sr.at[0], st_out)
     over_z = Direct(st2, Z, z, ss.at[1], sr.at[1])
@@ -415,6 +425,7 @@
     relay(1, 0)
     relay(2, 0)
     relay(3, 0)
+    pass_on(1)
     relay(1, 1)
     with scope("wait_y"):
         to_slices.arrive()
@@ -431,6 +442,7 @@
     over_z.start()
     relay(2, 1)
     relay(3, 1)
+    pass_on(2)
     relay(1, 2)
     with scope("wait_z"):
         over_z.arrive()
@@ -453,6 +465,7 @@
     shift = remote(rows_out, rows_in, ps.at[0], pr.at[0], {Z: after_z, Y: after_y})
     shift.start()
     relay(3, 2)
+    pass_on(3)
     with scope("proj_q"):
         query = (mm(scaled, g1a[0].reshape(D, DK)) * inv_rms).astype(BF16)
         query = query.astype(F32) * DK ** (-0.5)
@@ -502,27 +515,32 @@
         faded = query * jnp.exp(cum)
         y_pool = (mapped * silu(pgate)).astype(BF16)
     relay(3, 3)
+    pass_on(4)
     half_d = D // 2
 
     def project(left, weight, side):
         at = slice(side * (NR // 2), (side + 1) * (NR // 2))
-        return mm(left, weight[2, at].reshape(half_d, DK), 1, 1)
+        return mm(left.reshape(NX * OWN, DK), weight[at].reshape(half_d, DK), 1, 1)
+
+    def rows_copy(k):
+        return remote(yo.at[k], yi.at[k], bs.at[k], br.at[k], {C: other})
+
+    def give(k, value):
+        yb[k] = value.reshape(NX, 2, OWN, DK)
+        yo[k] = yb[k, :, other]
+        rows_copy(k).start()
 
     with scope("pooled"):
-        yb[...] = y_pool.reshape(NX, 2, OWN, DK)
-        for k, parity in enumerate((other, c)):
-            for side in range(2):
-                early[k, side] = project(yb[:, parity].reshape(NX * OWN, DK), g1b, side)
+        give(0, y_pool)
+        for side in range(2):
+            early[side] = project(yb[0, :, c], g1b.at[2], side)
     with scope("wait_back"):
         back.arrive()
     with scope("rec"):
         rec = rec + mm2(faded, st3[...].reshape(DK, DK), 1, 1)
         normed = rec * lax.rsqrt(jnp.mean(rec * rec, axis=1, keepdims=True) + EPS)
         y_rec = (normed * gate).astype(BF16)
-        yb[...] = y_rec.reshape(NX, 2, OWN, DK)
-
-    def sib_copy(side):
-        return remote(sib_out.at[side], sib_in.at[side], bs.at[0], br.at[side], {C: other})
+        give(1, y_rec)
 
     def red_copy(at, src, dst, step):
         return remote(src, dst, xs.at[0], xr.at[at], {X: around(x + step, NX)})
@@ -542,17 +560,20 @@
         ]
         for k in range(2)
     ]
-    with scope("proj_sib"):
-        for side in range(2):
-            part = early[0, side] + project(yb[:, other].reshape(NX * OWN, DK), g1a, side)
-            sib_out[side] = part.astype(BF16).reshape(NX, OWN, half_d)
-            sib_copy(side).start()
     with scope("proj_mine"):
         for side in range(2):
-            part = early[1, side] + project(yb[:, c].reshape(NX * OWN, DK), g1a, side)
-            part = part.reshape(NX, OWN, half_d)
-            sib_copy(side).wait_recv()
-            red_out[side] = (part + sib_in[side].astype(F32)).astype(BF16)
+            early[side] = early[side] + project(yb[1, :, c], g1a.at[2], side)
+    with scope("pooled_sib"):
+        remote(o2b, o2b, cs.at[1], cr.at[1], {C: other}).wait_recv()
+        rows_copy(0).wait_recv()
+        for side in range(2):
+            early[side] = early[side] + project(yi[0], o2b, side)
+    with scope("proj_sib"):
+        remote(o2a, o2a, cs.at[0], cr.at[0], {C: other}).wait_recv()
+        rows_copy(1).wait_recv()
+        for side in range(2):
+            part = early[side] + project(yi[1], o2a, side)
+            red_out[side] = part.astype(BF16).reshape(NX, OWN, half_d)
             for u in range(2):
                 over[side][u].start()
         for k in range(2):
@@ -581,7 +602,10 @@
             one.drain()
         seven = xg.at[pl.ds(0, 2 * NX - 1)]
         remote(seven, seven, ts.at[0], tr.at[0], {C: other}).wait_send()
-        remote(sib_out, sib_out, bs.at[0], br.at[0], {C: other}).wait_send()
+        for k in range(2):
+            rows_copy(k).wait_send()
+        remote(o2a, o2a, cs.at[0], cr.at[0], {C: other}).wait_send()
+        remote(o2b, o2b, cs.at[1], cr.at[1], {C: other}).wait_send()
         six = red_out.at[:, pl.ds(0, NX - 1)]
         remote(six, six, xs.at[0], xr.at[0], {X: right}).wait_send()
         shift.wait_send()
@@ -614,17 +638,19 @@
             pltpu.VMEM((DK, DK), BF16),
             pltpu.VMEM((1, DK), F32),
             pltpu.VMEM((1, D), F32),
-            pltpu.VMEM((NR, 32, DK), BF16),
-            pltpu.VMEM((NR, 32, DK), BF16),
-            pltpu.VMEM((NR, 32, DK), BF16),
+            pltpu.VMEM((NR, 24, DK), BF16),
+            pltpu.VMEM((NR, 24, DK), BF16),
+            pltpu.VMEM((NR, 24, DK), BF16),
             pltpu.VMEM((NR, 16, DK), BF16),
             pltpu.VMEM((NR, 16, DK), BF16),
             pltpu.VMEM((16, DK), BF16),
             pltpu.VMEM((16, DK), BF16),
-            pltpu.VMEM((NX, 2, OWN, DK), BF16),
-            pltpu.VMEM((2, 2, NX * OWN, D // 2), F32),
-            pltpu.VMEM((2, NX, OWN, D // 2), BF16),
-            pltpu.VMEM((2, NX, OWN, D // 2), BF16),
+            pltpu.VMEM((2, NX, 2, OWN, DK), BF16),
+            pltpu.VMEM((2, NX, OWN, DK), BF16),
+            pltpu.VMEM((2, NX, OWN, DK), BF16),
+            pltpu.VMEM((2, NX * OWN, D // 2), F32),
+            pltpu.VMEM((NR, NR, rows, DK), BF16),
+            pltpu.VMEM((NR, NR, rows, DK), BF16),
             pltpu.VMEM((2, NX, OWN, D // 2), BF16),
             pltpu.VMEM((4, OWN, D // 2), BF16),
             pltpu.VMEM((2, OWN, D // 2), BF16),
@@ -642,7 +668,9 @@
             dma((3,)),
             dma((1,)),
             dma((1,)),
-            dma((1,)),
+            dma((2,)),
+            dma((2,)),
+            dma((2,)),
             dma((2,)),
             dma((1,)),
             dma((5,)),

time: 59.2 us -> 58.7 us (level)
  Pallas kernels: 58.5 us -> 57.9 us
where the time goes in v7:
time: 58.7 us; the launch traced here: 58.6 us
  Pallas kernels  57.9 us (99%)
  local copies, waits for them, and re-layouts  0.66 us (1%)
    pallas_call x1, Pallas kernels, per_device(): run(*[pltpu.with_memory_space_constraint(a, pltpu.HBM) for a in operands])  57.9 us

profile of v7, /device:TPU:1, one launch (start us, length us, event | category | flops | bytes accessed | tf_op | source)
XLA Modules:
  0.0 58.6 jit_solution(7817790447969812292)
XLA Ops:
  0.0 57.9 %layer.1 = bf16[32,2048]{1,0:T(8,128)(2,1)S(1)} custom-call(bf16[256,256]{1,0:T(8,128)(2,1)} %tok.1, bf16[32,128]{1,0:T(8,128)(2,1)} %wq.1, bf16[32,128]{1,0:T(8,128)(2,1)} %wf.1, bf16[32,128]{1,0:T(8,128)(2,1)} %wi.1, bf16[32,128]{1,0:T(8,128)(2,1)} %wr.1, bf16[32,128]{1,0:T(8,128)(2,1)} %wp.1, bf16[32,128]{1,0:T(8,128)(2,1)} %wg.1, ...), custom_call_target="tpu_custom_call" | custom-call | tf_op jit(solution)/shard_map/layer/pallas_call | solution.py:700
  57.9 0.7 %copy.18 = bf16[32,2048]{1,0:T(8,128)(2,1)} copy(bf16[32,2048]{1,0:T(8,128)(2,1)S(1)} %layer.1) | data formatting | bytes 262144
